TPU v7x, 32 devices: a whole 2x2x4 slice. The times are simulated.
32 devices in a mesh: sp: 8 (over z, x), tp: 4 (over y, core).
Axes of the slice: x: 2, y: 2, z: 4, core: 2. Of those that a mesh axis runs over, the one named last changes fastest.
Arguments:
- stream: bfloat16 [1024, 2048], P('sp'), may hold values from -15 to 15
- cotangent: bfloat16 [1024, 2048], P('sp'), may hold values from -6 to 6
- route_ids: int32 [1024, 2], P('sp'), may hold values from 0 to 7, all different within a row; in each aligned block of 128 rows (0 to 127, 128 to 255, ...) at most 64 rows name the same one
- route_weights: float32 [1024, 2], P('sp'), may hold values from 0.1 to 0.9
- w_gate: bfloat16 [8, 2048, 2048], P('sp', None, 'tp'), may hold values from -0.125 to 0.125
- w_up: bfloat16 [8, 2048, 2048], P('sp', None, 'tp'), may hold values from -0.125 to 0.125
- w_down: bfloat16 [8, 2048, 2048], P('sp', 'tp'), may hold values from -0.125 to 0.125
- out_proj: bfloat16 [2048, 512], P(None, 'tp'), may hold values from -0.25 to 0.25
- mixed: bfloat16 [512, 1024], P('tp', 'sp'), may hold values from -6 to 6
- rec_input: bfloat16 [512, 1024], P('tp', 'sp'), may hold values from -6 to 6
- branch_input: bfloat16 [512, 1024], P('tp', 'sp'), may hold values from -6 to 6
- state_before: float32 [512, 1024], P('tp', 'sp'), may hold values from -6 to 6
- rec_gates: bfloat16 [16, 32, 32], P('tp'), may hold values from -1 to 1
- in_gates: bfloat16 [16, 32, 32], P('tp'), may hold values from -1 to 1
- decay_param: float32 [512], P('tp'), may hold values from 4.4 to 11
- decay_shift: float32 [512, 1024], P('tp', 'sp'), may hold values from -1.4 to -1e-05
Outputs:
- grad_gate: bfloat16 [8, 2048, 2048], P('sp', None, 'tp')
- grad_up: bfloat16 [8, 2048, 2048], P('sp', None, 'tp')
- grad_down: bfloat16 [8, 2048, 2048], P('sp', 'tp')
- grad_proj: float32 [2048, 512], P('sp', 'tp')
- grad_rec: float32 [512, 1024], P('tp', 'sp')
- grad_branch: float32 [512, 1024], P('tp', 'sp')
Inputs may be any that keep to these rules, and one draw needn't show every extreme that they name: `route_ids`: each row names 2 different experts; the rows of one device name no expert more than 64 times, a bound that some block reaches on some device.
All inputs are finite; a program needn't handle non-finite values.
Results may differ from a plain program's by a relative error of at most 0.03.
Values may be sent and summed in bfloat16 or wider, within the bound.
A program may use at most 64 MiB of HBM per device.

v0:
```python
import functools

import jax
import jax.numpy as jnp
from jax import lax
from jax.experimental import pallas as pl
from jax.experimental.pallas import tpu as pltpu
from jax.sharding import PartitionSpec as P

RATE_SCALE = 8.0
CLAMP_LIMIT = 7.0
GLU_ALPHA = 1.702
CORES = 2
MESH = pl.DeviceIdType.MESH
VMEM_LIMIT = 60 * 1024 * 1024


def expert_act(gate_pre, up_pre):
    glu_part = jnp.minimum(gate_pre, CLAMP_LIMIT)
    lin_part = jnp.clip(up_pre, -CLAMP_LIMIT, CLAMP_LIMIT)
    return glu_part * jax.nn.sigmoid(GLU_ALPHA * glu_part) * (lin_part + 1.0)


def reverse_step(later_elem, earlier_elem):
    return (later_elem[0] * earlier_elem[0], earlier_elem[1] + earlier_elem[0] * later_elem[1])


def weight_grads(tokens_in, grads_in, d_gate, d_up, act_low):
    g_gate = jnp.einsum("secd,secf->edf", tokens_in, d_gate, preferred_element_type=jnp.float32)
    g_up = jnp.einsum("secd,secf->edf", tokens_in, d_up, preferred_element_type=jnp.float32)
    g_down = jnp.einsum("secf,secd->efd", act_low, grads_in, preferred_element_type=jnp.float32)
    return (g_gate.astype(jnp.bfloat16), g_up.astype(jnp.bfloat16), g_down.astype(jnp.bfloat16))


def aligned(value, size):
    return pl.multiple_of(value * size, size)


def remote(src, dst, send_sem, recv_sem, device):
    return pltpu.make_async_remote_copy(
        src_ref=src,
        dst_ref=dst,
        send_sem=send_sem,
        recv_sem=recv_sem,
        device_id=device,
        device_id_type=MESH,
    )


class Place:
    def __init__(self, n_sp, n_tp):
        self.n, self.ny = n_sp, n_tp // CORES
        self.s, self.t = lax.axis_index("sp"), lax.axis_index("tp")
        self.y, self.c = self.t // CORES, lax.rem(self.t, CORES)
        self.partner = (self.s, self.y * CORES + 1 - self.c)

    def sp_peer(self, i):
        return lax.rem(self.s + i, self.n)

    def sp_source(self, i):
        return lax.rem(self.s + self.n - i, self.n)

    def mirror(self, i):
        found, bit = 0, 1
        while bit < self.n:
            found = found + lax.rem(self.s // bit + i // bit, 2) * bit
            bit *= 2
        return found

    def y_peer(self, j):
        return lax.rem(self.y + j, self.ny)

    def y_source(self, j):
        return lax.rem(self.y + self.ny - j, self.ny)

    def tp_of(self, y, c):
        return y * CORES + c

    def barrier(self, along_tp=True):
        sem = pltpu.get_barrier_semaphore()

        def greet(device):
            pl.semaphore_signal(sem, inc=1, device_id=device, device_id_type=MESH)

        for i in range(1, self.n):
            greet((self.sp_peer(i), self.t))
        count = self.n - 1
        if along_tp:
            for j in range(1, self.ny):
                greet((self.s, self.tp_of(self.y_peer(j), self.c)))
            greet(self.partner)
            count += self.ny
        pl.semaphore_wait(sem, count)


def dispatch_kernel(
    n_sp, n_tp, tok_src, grd_src, tok_near, grd_near, tok_out, grd_out,
    own_sem, sa, ra, sy, ry, sc, rc, sd,
):
    at = Place(n_sp, n_tp)
    rows = tok_src.shape[0] // n_sp
    cols = tok_src.shape[1]
    pairs = ((tok_src, tok_out), (grd_src, grd_out))
    nears = (tok_near, grd_near)
    near, near_from = at.mirror(1), 1

    def block(out, source, tp):
        return out.at[pl.ds(aligned(source, rows), rows), pl.ds(aligned(tp, cols), cols)]

    def first(a, i):
        src, out = pairs[a]
        peer = at.mirror(i)
        return remote(
            src.at[pl.ds(aligned(peer, rows), rows), :],
            block(out, at.s, at.t),
            sa.at[a, i],
            ra.at[a, i],
            (peer, at.t),
        )

    def along_y(a, i, j, source, outgoing):
        src, out = pairs[a]
        tp = at.t if outgoing else at.tp_of(at.y_source(j), at.c)
        spot = block(out, source, tp)
        return remote(
            spot, spot, sy.at[a, i, j], ry.at[a, i, j], (at.s, at.tp_of(at.y_peer(j), at.c))
        )

    def across(a, i, j, source, outgoing):
        src, out = pairs[a]
        tp = at.tp_of(at.y_source(j), at.c if outgoing else 1 - at.c)
        spot = block(out, source, tp)
        return remote(spot, spot, sc.at[a, i, j], rc.at[a, i, j], at.partner)

    def direct(a, j):
        tp = at.tp_of(at.y_source(j), at.c)
        return remote(
            nears[a].at[pl.ds(rows, rows), pl.ds(aligned(tp, cols), cols)],
            block(pairs[a][1], at.s, tp),
            sd.at[a, j],
            ry.at[a, near_from, j],
            (near, at.t),
        )

    own = []
    for a in range(2):
        copy = pltpu.make_async_copy(
            nears[a].at[pl.ds(0, rows), :],
            pairs[a][1].at[pl.ds(aligned(at.s, rows), rows), :],
            own_sem.at[a],
        )
        copy.start()
        own.append(copy)
    at.barrier()

    def send(i, _):
        for a in range(2):
            first(a, i).start()
        return 0

    lax.fori_loop(1, n_sp, send, 0)
    for a in range(2):
        for j in range(1, at.ny):
            direct(a, j).start()

    def pass_on(a, i):
        source = at.mirror(i)

        @pl.when(i != near_from)
        def _():
            for j in range(1, at.ny):
                along_y(a, i, j, source, True).start()

        across(a, i, 0, source, True).start()

    def relay(a, i):
        source = at.mirror(i)
        for j in range(1, at.ny):
            along_y(a, i, j, source, False).wait_recv()
            across(a, i, j, source, True).start()

    for a in range(2):
        first(a, 1).wait_recv()
        pass_on(a, 1)

    def step(i, _):
        for a in range(2):
            first(a, i).wait_recv()
            pass_on(a, i)
        for a in range(2):
            relay(a, i - 1)
        return 0

    lax.fori_loop(2, n_sp, step, 0)
    for a in range(2):
        relay(a, n_sp - 1)

    for a in range(2):

        def drain(i, _):
            source = at.mirror(i)
            for j in range(at.ny):
                across(a, i, j, source, False).wait_recv()
                across(a, i, j, source, True).wait_send()

            @pl.when(i != near_from)
            def _():
                for j in range(1, at.ny):
                    along_y(a, i, j, source, True).wait_send()

            first(a, i).wait_send()
            return 0

        lax.fori_loop(1, n_sp, drain, 0)
        for j in range(1, at.ny):
            direct(a, j).wait_send()
        own[a].wait()


def dispatch(tok_src, grd_src, tok_near, grd_near, n_sp, n_tp):
    total, cols = tok_src.shape
    ny = n_tp // CORES
    dma = pltpu.SemaphoreType.DMA
    shape = jax.ShapeDtypeStruct((total, cols * n_tp), jnp.bfloat16)
    return pl.pallas_call(
        functools.partial(dispatch_kernel, n_sp, n_tp),
        out_shape=(shape, shape),
        in_specs=[pl.BlockSpec(memory_space=pltpu.VMEM)] * 4,
        out_specs=[pl.BlockSpec(memory_space=pl.ANY)] * 2,
        scratch_shapes=[
            dma((2,)),
            dma((2, n_sp)),
            dma((2, n_sp)),
            dma((2, n_sp, ny)),
            dma((2, n_sp, ny)),
            dma((2, n_sp, ny)),
            dma((2, n_sp, ny)),
            dma((2, ny)),
        ],
        compiler_params=pltpu.CompilerParams(
            collective_id=0, has_side_effects=True, vmem_limit_bytes=VMEM_LIMIT
        ),
    )(tok_src, grd_src, tok_near, grd_near)


def return_kernel(
    n_sp, n_tp, part, pick, cot, out,
    core_in, own_sum, y_out, y_in, ret_out, ret_in, low,
    sc, rc, sy, ry, sr, rr, sl, rl, sp_, rp_, own_sem,
):
    at = Place(n_sp, n_tp)
    rows = part.shape[0] // n_sp
    cols = part.shape[1] // n_tp
    tok = cot.shape[0]

    def piece(peer, tp):
        return pl.ds(aligned(peer, rows), rows), pl.ds(aligned(tp, cols), cols)

    def peer_of(i):
        return at.mirror(n_sp - 1 - i)

    def core_copy(i, j):
        r, c = piece(peer_of(i), at.tp_of(at.y_peer(j), 1 - at.c))
        return remote(part.at[r, c], core_in.at[i, j], sc.at[i, j], rc.at[i, j], at.partner)

    def y_copy(i, j):
        return remote(
            y_out.at[i, j],
            y_in.at[i, j],
            sy.at[i, j],
            ry.at[i, j],
            (at.s, at.tp_of(at.y_peer(j), at.c)),
        )

    def home_copy(i):
        return remote(
            ret_out.at[i],
            ret_in.at[pl.ds(aligned(at.s, rows), rows), :],
            sr.at[i],
            rr.at[i],
            (peer_of(i), at.t),
        )

    at.barrier()

    def send_core(i, _):
        for j in range(at.ny):
            core_copy(i, j).start()
        return 0

    lax.fori_loop(0, n_sp, send_core, 0)

    def reduce_core(i):
        peer = peer_of(i)
        for j in list(range(1, at.ny)) + [0]:
            core_copy(i, j).wait_recv()
            r, c = piece(peer, at.tp_of(at.y_peer(j), at.c))
            both = part[r, c].astype(jnp.float32) + core_in[i, j].astype(jnp.float32)
            if j:
                y_out[i, j] = both.astype(jnp.bfloat16)
                y_copy(i, j).start()
            else:
                own_sum[i] = both

    def reduce_y(i):
        total = own_sum[i]
        for j in range(1, at.ny):
            y_copy(i, j).wait_recv()
            total = total + y_in[i, j].astype(jnp.float32)
        return total.astype(jnp.bfloat16)

    def send_home(i):
        ret_out[i] = reduce_y(i)
        home_copy(i).start()

    reduce_core(0)

    def step(i, _):
        reduce_core(i)
        send_home(i - 1)
        return 0

    lax.fori_loop(1, n_sp, step, 0)
    ret_in[pl.ds(aligned(at.s, rows), rows), :] = reduce_y(n_sp - 1)

    def wait_home(i, _):
        source = peer_of(i)
        spot = ret_in.at[pl.ds(aligned(source, rows), rows), :]
        remote(ret_out.at[i], spot, sr.at[i], rr.at[i], (peer_of(i), at.t)).wait_recv()
        return 0

    lax.fori_loop(0, n_sp - 1, wait_home, 0)
    own_cols = cot[:, pl.ds(aligned(at.t, cols), cols)].astype(jnp.float32)
    pair_sum = jnp.dot(pick[...], ret_in[...], preferred_element_type=jnp.float32)
    low[...] = (own_cols + pair_sum).astype(jnp.bfloat16)

    def spot_of(tp):
        return out.at[:, pl.ds(aligned(tp, cols), cols)]

    def low_y(j):
        return remote(
            low, spot_of(at.t), sl.at[j], rl.at[j], (at.s, at.tp_of(at.y_peer(j), at.c))
        )

    def low_y_in(j):
        return remote(
            low,
            spot_of(at.tp_of(at.y_source(j), at.c)),
            sl.at[j],
            rl.at[j],
            (at.s, at.tp_of(at.y_peer(j), at.c)),
        )

    def low_core(j, outgoing):
        spot = spot_of(at.tp_of(at.y_source(j), at.c if outgoing else 1 - at.c))
        src = low if j == 0 else spot
        return remote(src, spot, sp_.at[j], rp_.at[j], at.partner)

    for j in range(1, at.ny):
        low_y(j).start()
    low_core(0, True).start()
    own = pltpu.make_async_copy(low, spot_of(at.t), own_sem)
    own.start()
    for j in range(1, at.ny):
        low_y_in(j).wait_recv()
        low_core(j, True).start()
    own.wait()
    for j in range(at.ny):
        low_core(j, False).wait_recv()
        low_core(j, True).wait_send()
    for j in range(1, at.ny):
        low_y(j).wait_send()

    def drain(i, _):
        for j in range(at.ny):
            core_copy(i, j).wait_send()
        for j in range(1, at.ny):
            y_copy(i, j).wait_send()
        return 0

    def drain_home(i, _):
        home_copy(i).wait_send()
        return 0

    lax.fori_loop(0, n_sp, drain, 0)
    lax.fori_loop(0, n_sp - 1, drain_home, 0)


def give_back(part, pick, cot, n_sp, n_tp):
    total, width = part.shape
    rows, cols, ny, tok = total // n_sp, width // n_tp, n_tp // CORES, cot.shape[0]
    dma = pltpu.SemaphoreType.DMA
    bf = jnp.bfloat16
    return pl.pallas_call(
        functools.partial(return_kernel, n_sp, n_tp),
        out_shape=jax.ShapeDtypeStruct((tok, width), bf),
        in_specs=[pl.BlockSpec(memory_space=pltpu.VMEM)] * 3,
        out_specs=pl.BlockSpec(memory_space=pltpu.VMEM),
        scratch_shapes=[
            pltpu.VMEM((n_sp, ny, rows, cols), bf),
            pltpu.VMEM((n_sp, rows, cols), jnp.float32),
            pltpu.VMEM((n_sp, ny, rows, cols), bf),
            pltpu.VMEM((n_sp, ny, rows, cols), bf),
            pltpu.VMEM((n_sp, rows, cols), bf),
            pltpu.VMEM((n_sp * rows, cols), bf),
            pltpu.VMEM((tok, cols), bf),
            dma((n_sp, ny)),
            dma((n_sp, ny)),
            dma((n_sp, ny)),
            dma((n_sp, ny)),
            dma((n_sp,)),
            dma((n_sp,)),
            dma((ny,)),
            dma((ny,)),
            dma((ny,)),
            dma((ny,)),
            dma,
        ],
        compiler_params=pltpu.CompilerParams(
            collective_id=1, has_side_effects=True, vmem_limit_bytes=VMEM_LIMIT
        ),
    )(part, pick, cot)


def close_kernel(n_sp, n_tp, part, link, proj, carry, held, links, sg, rg, sk, rk):
    at = Place(n_sp, n_tp)
    rows = part.shape[0] // n_sp

    def proj_copy(i):
        peer = at.mirror(i)
        return remote(
            part.at[pl.ds(aligned(peer, rows), rows), :],
            held.at[i],
            sg.at[i],
            rg.at[i],
            (peer, at.t),
        )

    def link_copy(i):
        return remote(link, links.at[i], sk.at[i], rk.at[i], (at.sp_peer(i), at.t))

    at.barrier(False)

    def send_link(i, _):
        link_copy(i).start()
        return 0

    def send_proj(i, _):
        proj_copy(n_sp - i).start()
        return 0

    lax.fori_loop(1, n_sp, send_link, 0)
    lax.fori_loop(1, n_sp, send_proj, 0)

    def compose(k, state):
        i = k + 1
        link_copy(i).wait_recv()
        ahead = n_sp - i
        later = at.s + ahead < n_sp
        lower = links[i]
        return jnp.where(later, lower[0:1] * state + lower[1:2], state)

    carry[...] = lax.fori_loop(0, n_sp - 1, compose, jnp.zeros(carry.shape, jnp.float32))

    proj[...] = part[pl.ds(aligned(at.s, rows), rows), :].astype(jnp.float32)

    def add(i, _):
        proj_copy(i).wait_recv()
        proj[...] += held[i].astype(jnp.float32)
        return 0

    lax.fori_loop(1, n_sp, add, 0)

    def drain(i, _):
        link_copy(i).wait_send()
        proj_copy(i).wait_send()
        return 0

    lax.fori_loop(1, n_sp, drain, 0)


def close(part, link, n_sp, n_tp):
    total, channels = part.shape
    dma = pltpu.SemaphoreType.DMA
    return pl.pallas_call(
        functools.partial(close_kernel, n_sp, n_tp),
        out_shape=(
            jax.ShapeDtypeStruct((total // n_sp, channels), jnp.float32),
            jax.ShapeDtypeStruct((1, channels), jnp.float32),
        ),
        in_specs=[pl.BlockSpec(memory_space=pltpu.VMEM)] * 2,
        out_specs=[pl.BlockSpec(memory_space=pltpu.VMEM)] * 2,
        scratch_shapes=[
            pltpu.VMEM((n_sp, total // n_sp, channels), jnp.bfloat16),
            pltpu.VMEM((n_sp,) + link.shape, jnp.float32),
            dma((n_sp,)),
            dma((n_sp,)),
            dma((n_sp,)),
            dma((n_sp,)),
        ],
        compiler_params=pltpu.CompilerParams(
            collective_id=2, has_side_effects=True, vmem_limit_bytes=VMEM_LIMIT
        ),
    )(part, link)


def local(
    stream,
    cotangent,
    route_ids,
    route_weights,
    w_gate,
    w_up,
    w_down,
    out_proj,
    mixed,
    rec_input,
    branch_input,
    state_before,
    rec_gates,
    in_gates,
    decay_param,
    decay_shift,
):
    sp_count, tp_count = lax.axis_size("sp"), lax.axis_size("tp")
    tok_rows, model_width = cotangent.shape
    top_count = route_ids.shape[1]
    local_experts = w_gate.shape[0]
    expert_count = local_experts * sp_count
    capacity = 2 * tok_rows * top_count // expert_count
    slots = expert_count * capacity
    share_cols = model_width // tp_count
    flat_ids = route_ids.reshape(-1)
    pair_at = jnp.arange(flat_ids.shape[0], dtype=jnp.int32)
    earlier = (flat_ids[:, None] == flat_ids[None, :]) & (pair_at[None, :] < pair_at[:, None])
    slot_index = jnp.sum(earlier.astype(jnp.int32), axis=1)
    target = (flat_ids * capacity + slot_index).reshape(tok_rows, top_count)
    slot_at = jnp.arange(slots, dtype=jnp.int32)
    pick = functools.reduce(
        jnp.logical_or, [target[:, k][:, None] == slot_at[None, :] for k in range(top_count)]
    ).astype(jnp.bfloat16)
    first_col = lax.axis_index("tp") * share_cols
    own_stream = lax.dynamic_slice_in_dim(stream, first_col, share_cols, 1)
    own_cot = lax.dynamic_slice_in_dim(cotangent, first_col, share_cols, 1)
    place = lax.axis_index("sp")
    chunk = slots // sp_count
    near_at = jnp.concatenate(
        [place * chunk + slot_at[:chunk], (place + 1 - 2 * (place % 2)) * chunk + slot_at[:chunk]]
    )

    def to_slots(at, rows_in, cot_in):
        lands = [target[:, k][None, :] == at[:, None] for k in range(top_count)]
        lands_any = functools.reduce(jnp.logical_or, lands).astype(jnp.bfloat16)
        scaled = [
            (route_weights[:, k : k + 1] * cot_in.astype(jnp.float32)).astype(jnp.bfloat16)
            for k in range(top_count)
        ]
        tokens = jnp.dot(lands_any, rows_in, preferred_element_type=jnp.float32)
        grads = jnp.dot(
            jnp.concatenate(lands, axis=1).astype(jnp.bfloat16),
            jnp.concatenate(scaled, axis=0),
            preferred_element_type=jnp.float32,
        )
        return tokens.astype(jnp.bfloat16), grads.astype(jnp.bfloat16)

    tok_src, grd_src = to_slots(slot_at, own_stream, own_cot)
    tok_near, grd_near = to_slots(near_at, stream, cotangent)
    tokens_in, grads_in = dispatch(tok_src, grd_src, tok_near, grd_near, sp_count, tp_count)
    grads_in = grads_in.reshape(sp_count, local_experts, capacity, model_width)
    tokens_in = tokens_in.reshape(sp_count, local_experts, capacity, model_width)
    gate_pre = jnp.einsum("secd,edf->secf", tokens_in, w_gate, preferred_element_type=jnp.float32)
    up_pre = jnp.einsum("secd,edf->secf", tokens_in, w_up, preferred_element_type=jnp.float32)
    act_val, act_vjp = jax.vjp(expert_act, gate_pre, up_pre)
    act_low = act_val.astype(jnp.bfloat16)
    d_act = jnp.einsum("secd,efd->secf", grads_in, w_down, preferred_element_type=jnp.float32)
    d_gate, d_up = act_vjp(d_act)
    d_gate = d_gate.astype(jnp.bfloat16)
    d_up = d_up.astype(jnp.bfloat16)
    grad_gate, grad_up, grad_down = weight_grads(tokens_in, grads_in, d_gate, d_up, act_low)
    partial_value = jnp.einsum("secf,edf->secd", d_gate, w_gate, preferred_element_type=jnp.float32)
    partial_value = partial_value + jnp.einsum(
        "secf,edf->secd", d_up, w_up, preferred_element_type=jnp.float32
    )
    partial_low = partial_value.astype(jnp.bfloat16).reshape(slots, model_width)
    stream_low = give_back(partial_low, pick, cotangent, sp_count, tp_count)
    d_mixed = lax.dot_general(
        out_proj, stream_low, (((0,), (1,)), ((), ())), preferred_element_type=jnp.float32
    )
    proj_part = lax.dot_general(
        stream_low, mixed, (((0,), (1,)), ((), ())), preferred_element_type=jnp.float32
    ).astype(jnp.bfloat16)
    channels, positions = rec_input.shape
    gate_heads = rec_gates.shape[0]
    head_dim = rec_gates.shape[1]
    rec_heads = rec_input.reshape(gate_heads, head_dim, positions)
    rec_pre = jnp.einsum(
        "hij,hit->hjt", rec_gates, rec_heads, preferred_element_type=jnp.float32
    ).reshape(channels, positions)
    in_pre = jnp.einsum(
        "hij,hit->hjt", in_gates, rec_heads, preferred_element_type=jnp.float32
    ).reshape(channels, positions)
    rec_gate = jax.nn.sigmoid(rec_pre)
    in_gate = jax.nn.sigmoid(in_pre)
    soft_plus = jax.nn.softplus(-decay_param)[:, None]
    log_decay = -RATE_SCALE * rec_gate * soft_plus + decay_shift
    decay_rate = jnp.exp(log_decay)
    token_position = lax.axis_index("sp") * positions + jnp.arange(positions, dtype=jnp.int32)
    at_start = (token_position == 0)[None, :]
    raw_mult = jnp.sqrt(-jnp.expm1(2.0 * log_decay))
    multiplier = jnp.where(at_start, 1.0, raw_mult)
    rec_value = rec_input.astype(jnp.float32)
    state_now = decay_rate * state_before + multiplier * in_gate * rec_value
    gelu_val, gelu_vjp = jax.vjp(jax.nn.gelu, branch_input.astype(jnp.float32))
    grad_branch = gelu_vjp(d_mixed * state_now)[0]
    d_state = d_mixed * gelu_val
    next_decay = jnp.concatenate([decay_rate[:, 1:], jnp.zeros((channels, 1), jnp.float32)], axis=1)
    local_adj = lax.associative_scan(reverse_step, (next_decay, d_state), reverse=True, axis=1)[1]
    log_cumsum = jnp.cumsum(log_decay, axis=1)
    total_log = log_cumsum[:, -1:]
    tail_decay = jnp.exp(total_log - log_cumsum)
    device_prod = jnp.exp(total_log[:, 0])
    head_term = decay_rate[:, 0] * local_adj[:, 0]
    link = jnp.concatenate(
        [device_prod[None], head_term[None], jnp.zeros((6, channels), jnp.float32)], axis=0
    )
    grad_proj, carried = close(proj_part, link, sp_count, tp_count)
    adjoint = local_adj + tail_decay * carried[0][:, None]
    mult_term = adjoint * in_gate * rec_value * decay_rate * decay_rate / raw_mult
    d_log = adjoint * state_before * decay_rate - jnp.where(at_start, 0.0, mult_term)
    d_rec_pre = (d_log * -RATE_SCALE * soft_plus * rec_gate * (1.0 - rec_gate)).astype(jnp.bfloat16)
    d_in_pre = (adjoint * multiplier * rec_value * in_gate * (1.0 - in_gate)).astype(jnp.bfloat16)
    back_rec = jnp.einsum(
        "hij,hjt->hit",
        rec_gates,
        d_rec_pre.reshape(gate_heads, head_dim, positions),
        preferred_element_type=jnp.float32,
    )
    back_in = jnp.einsum(
        "hij,hjt->hit",
        in_gates,
        d_in_pre.reshape(gate_heads, head_dim, positions),
        preferred_element_type=jnp.float32,
    )
    grad_rec = adjoint * multiplier * in_gate + (back_rec + back_in).reshape(channels, positions)
    return (grad_gate, grad_up, grad_down, grad_proj, grad_rec, grad_branch)


def solution(mesh):
    placed = (
        P("sp", None),
        P("sp", None),
        P("sp", None),
        P("sp", None),
        P("sp", None, "tp"),
        P("sp", None, "tp"),
        P("sp", "tp", None),
        P(None, "tp"),
        P("tp", "sp"),
        P("tp", "sp"),
        P("tp", "sp"),
        P("tp", "sp"),
        P("tp", None, None),
        P("tp", None, None),
        P("tp"),
        P("tp", "sp"),
    )
    return jax.shard_map(
        local,
        mesh=mesh,
        in_specs=placed,
        out_specs=(
            P("sp", None, "tp"),
            P("sp", None, "tp"),
            P("sp", "tp", None),
            P("sp", "tp"),
            P("tp", "sp"),
            P("tp", "sp"),
        ),
        check_vma=False,
    )
```

profile of v0, /device:TPU:0, one launch (start us, length us, event | category | flops | bytes accessed | tf_op | source)
XLA Modules:
  0.0 132.2 jit_solution(7602574527430533400)
XLA Ops:
  0.6 0.0 copy-start
  0.6 0.0 copy-start.4
  0.7 0.0 copy-start.2
  0.7 0.9 copy.111
  1.6 0.1 eq.133
  1.8 0.2 convert_reduce_fusion
  1.9 0.1 reduce_sum.12
  2.1 0.1 copy.112
  2.2 0.7 multiply_add_fusion.11
  2.9 2.0 %convolution_convert_fusion.4.tok_src = bf16[512,512]{1,0:T(8,128)(2,1)} fusion(bf16[128,2048]{1,0:T(8,128)(2,1)} %param.16, s32[]{:T(128)S(6)} %select_n.73, s32[128]{0:T(128)S(1)} %get-tuple-element.79, s32[128]{0:T(128)S(1)} %get-tuple-element.78), kind=kOutput, calls=%fused_computation.24 | convolution fusion | flops 67567616 | bytes 656388 | tf_op jit(solution)/shard_map/dot_general | solution.py:558
  4.9 0.1 iota_compare_fusion.2
  4.9 0.8 slice_bitcast_fusion.1
  5.7 1.0 fusion.49
  6.7 1.1 convolution_convert_fusion.3.grd_src
  7.8 0.1 pad_add_fusion.1
  7.9 1.1 convolution_convert_fusion.2.tok_near
  9.1 0.2 fusion.21
  9.3 0.1 broadcast_compare_fusion.1
  9.4 1.1 convolution_convert_fusion.1.grd_near
  10.5 37.7 %shard_map.199 = (bf16[512,2048]{1,0:T(8,128)(2,1)}, bf16[512,2048]{1,0:T(8,128)(2,1)}) custom-call(bf16[512,512]{1,0:T(8,128)(2,1)} %convolution_convert_fusion.4.tok_src, bf16[512,512]{1,0:T(8,128)(2,1)} %convolution_convert_fusion.3.grd_src, bf16[128,2048]{1,0:T(8,128)(2,1)} %convolution_convert_fusion.2.tok_near, ...), custom_call_target="tpu_custom_call" | custom-call | tf_op jit(solution)/shard_map/pallas_call | solution.py:225
  48.2 0.0 copy-start.18
  48.2 3.6 %fusion.8 = f32[8,64,512]{2,1,0:T(8,128)S(1)} fusion(bf16[8,64,2048]{2,1,0:T(8,128)(2,1)} %bitcast.184, bf16[1,2048,512]{2,1,0:T(8,128)(2,1)} %param.21), kind=kOutput, calls=%fused_computation.15 | convolution fusion | flops 1073741824 | bytes 5242880 | tf_op jit(solution)/shard_map/secd,edf->secf/dot_general | solution.py:572
  51.9 0.0 copy-start.16
  51.9 1.3 fusion.5
  53.1 0.3 copy-done.16
  53.4 0.6 copy-done.17
  54.1 2.3 %fusion.31 = (bf16[8,1,64,512]{3,2,0,1:T(8,128)(2,1)S(1)}, bf16[8,1,64,512]{3,2,0,1:T(8,128)(2,1)S(1)}) fusion(f32[8,64,512]{2,1,0:T(8,128)S(1)} %fusion.8, f32[8,64,512]{2,1,0:T(8,128)S(1)} %fusion.5, bf16[8,64,2048]{2,1,0:T(8,128)(2,1)S(1)} %bitcast.182, bf16[1,512,2048]{2,1,0:T(8,128)(2,1)S(1)} %copy-done.16), kind=kOutput, calls=%fused_computation.46 | convolution fusion | flops 1082916864 | bytes 7340032 | tf_op jit(solution)/shard_map/secd,efd->secf/dot_general | solution.py:575
  56.3 2.6 %fusion = bf16[1,2048,512]{2,1,0:T(8,128)(2,1)} fusion(bf16[8,64,2048]{2,1,0:T(8,128)(2,1)S(1)} %bitcast.186, bf16[8,1,64,512]{3,2,0,1:T(8,128)(2,1)S(1)} %get-tuple-element.49), kind=kOutput, calls=%fused_computation.4 | convolution fusion | flops 1074790400 | bytes 4718592 | tf_op jit(solution)/shard_map/secd,secf->edf/dot_general | solution.py:29
  59.0 2.6 %fusion.1 = bf16[1,2048,512]{2,1,0:T(8,128)(2,1)} fusion(bf16[8,64,2048]{2,1,0:T(8,128)(2,1)S(1)} %bitcast.187, bf16[8,1,64,512]{3,2,0,1:T(8,128)(2,1)S(1)} %get-tuple-element.48), kind=kOutput, calls=%fused_computation.5 | convolution fusion | flops 1074790400 | bytes 4718592 | tf_op jit(solution)/shard_map/secd,secf->edf/dot_general | solution.py:30
  61.6 2.8 %fusion.2 = bf16[1,512,2048]{2,1,0:T(8,128)(2,1)} fusion(bf16[8,64,2048]{2,1,0:T(8,128)(2,1)S(1)} %bitcast.183, f32[8,64,512]{2,1,0:T(8,128)S(1)} %fusion.8, f32[8,64,512]{2,1,0:T(8,128)S(1)} %fusion.5), kind=kOutput, calls=%fused_computation.6 | convolution fusion | flops 1077411840 | bytes 6291456 | tf_op jit(solution)/shard_map/secf,secd->efd/dot_general | solution.py:31
  64.4 1.3 fusion.3
  65.7 0.3 copy-done.3
  66.0 2.6 %add_convert_fusion = bf16[8,64,2048]{2,1,0:T(8,128)(2,1)} fusion(f32[8,64,2048]{2,1,0:T(8,128)S(1)} %fusion.3, bf16[1,2048,512]{2,1,0:T(8,128)(2,1)S(1)} %copy-done.3, bf16[8,1,64,512]{3,2,0,1:T(8,128)(2,1)S(1)} %get-tuple-element.48), kind=kOutput, calls=%fused_computation.3 | convolution fusion | flops 1075838976 | bytes 8912896 | tf_op jit(solution)/shard_map/secf,edf->secd/dot_general | solution.py:581
  68.6 0.8 fusion.56.pick
  69.4 0.0 copy-start.13
  69.4 0.0 copy-start.19
  69.4 0.0 copy-start.5
  69.4 31.6 %shard_map.200 = bf16[128,2048]{1,0:T(8,128)(2,1)} custom-call(bf16[512,2048]{1,0:T(8,128)(2,1)} %bitcast.173, bf16[128,512]{1,0:T(8,128)(2,1)} %fusion.56.pick, bf16[128,2048]{1,0:T(8,128)(2,1)} %cot.1), custom_call_target="tpu_custom_call" | custom-call | tf_op jit(solution)/shard_map/pallas_call | solution.py:394
  101.0 2.2 %convolution_convert_fusion.part = bf16[2048,128]{1,0:T(8,128)(2,1)} fusion(bf16[128,2048]{1,0:T(8,128)(2,1)} %shard_map.200, bf16[128,128]{1,0:T(8,128)(2,1)S(1)} %copy-done.10), kind=kOutput, calls=%fused_computation.7 | convolution fusion | flops 67371008 | bytes 1081344 | tf_op jit(solution)/shard_map/dot_general | solution.py:589
  103.2 0.1 copy.116
  103.4 0.1 copy.121
  103.5 1.0 fusion.17
  104.5 0.1 copy.118
  104.6 0.1 copy.119
  104.7 0.7 copy.115
  105.4 0.2 fusion.20
  105.6 0.1 copy.114
  105.8 1.8 %fusion.64 = (f32[128,128]{0,1:T(8,128)}, f32[128,128]{0,1:T(8,128)S(1)}, f32[128,128]{0,1:T(8,128)S(1)}) fusion(bf16[128,128]{0,1:T(8,128)(2,1)S(1)} %copy.116, bf16[128,128]{0,1:T(8,128)(2,1)S(1)} %copy.121, f32[128,128]{0,1:T(8,128)S(1)} %copy.118, f32[128,128]{0,1:T(8,128)S(1)} %copy.119, pred[128]{0:T(512)(128)(4,1)S(1)} %add_compare_fusion, ...), kind=kOutput, calls=%fused_computation.102 | convolution fusion | flops 67649536 | bytes 1573504 | tf_op jit(solution)/shard_map/dot_general | solution.py:586
  107.7 0.0 copy-start.14
  107.7 0.0 copy-start.15
  107.9 0.0 copy-start.6
  108.9 0.2 reduce_window_sum.11
  109.1 0.1 pad.61.clone
  109.2 0.7 maximum_maximum_fusion.link
  109.9 18.7 %shard_map.201 = (f32[256,128]{1,0:T(8,128)}, f32[1,128]{1,0:T(1,128)}) custom-call(bf16[2048,128]{1,0:T(8,128)(2,1)} %convolution_convert_fusion.part, f32[8,128]{1,0:T(8,128)} %maximum_maximum_fusion.link), custom_call_target="tpu_custom_call" | custom-call | tf_op jit(solution)/shard_map/pallas_call | solution.py:485
  128.7 0.8 fusion.67
  129.4 0.1 copy.124
  129.5 0.1 fusion.105
  129.7 0.1 copy.127
  129.8 0.1 convolution_add_fusion
  129.9 0.1 copy.128
  130.0 0.7 copy.131
  130.8 0.7 copy.132
  131.5 0.7 copy.144
  (122 shorter events, 1.1 us)
Async XLA Ops:
  0.6 51.2 %copy-start = (bf16[1,2048,512]{2,1,0:T(8,128)(2,1)S(1)}, bf16[1,2048,512]{2,1,0:T(8,128)(2,1)}, u32[]{:S(2)}) copy-start(bf16[1,2048,512]{2,1,0:T(8,128)(2,1)} %param.20) | copy-start | bytes 6291460
  0.6 7.3 %copy-start.4 = (bf16[128,2048]{1,0:T(8,128)(2,1)S(1)}, bf16[128,2048]{1,0:T(8,128)(2,1)}, u32[]{:S(2)}) copy-start(bf16[128,2048]{1,0:T(8,128)(2,1)} %param.16) | copy-start | bytes 1572868
  0.7 8.4 %copy-start.2 = (bf16[128,2048]{1,0:T(8,128)(2,1)S(1)}, bf16[128,2048]{1,0:T(8,128)(2,1)}, u32[]{:S(2)}) copy-start(bf16[128,2048]{1,0:T(8,128)(2,1)} %cot.1) | copy-start | bytes 1572868
  48.2 3.6 %copy-start.18 = (bf16[512,2048]{1,0:T(8,128)(2,1)S(1)}, bf16[512,2048]{1,0:T(8,128)(2,1)}, u32[]{:S(2)}) copy-start(bf16[512,2048]{1,0:T(8,128)(2,1)} %get-tuple-element.10) | copy-start | bytes 6291460
  51.9 1.6 %copy-start.16 = (bf16[1,512,2048]{2,1,0:T(8,128)(2,1)S(1)}, bf16[1,512,2048]{2,1,0:T(8,128)(2,1)}, u32[]{:S(2)}) copy-start(bf16[1,512,2048]{2,1,0:T(8,128)(2,1)} %param.22) | copy-start | bytes 6291460
  51.9 2.2 %copy-start.17 = (bf16[512,2048]{1,0:T(8,128)(2,1)S(1)}, bf16[512,2048]{1,0:T(8,128)(2,1)}, u32[]{:S(2)}) copy-start(bf16[512,2048]{1,0:T(8,128)(2,1)} %get-tuple-element.11) | copy-start | bytes 6291460
  64.4 1.6 %copy-start.3 = (bf16[1,2048,512]{2,1,0:T(8,128)(2,1)S(1)}, bf16[1,2048,512]{2,1,0:T(8,128)(2,1)}, u32[]{:S(2)}) copy-start(bf16[1,2048,512]{2,1,0:T(8,128)(2,1)} %param.21) | copy-start | bytes 6291460
  68.6 32.4 %copy-start.10 = (bf16[128,128]{1,0:T(8,128)(2,1)S(1)}, bf16[128,128]{1,0:T(8,128)(2,1)}, u32[]{:S(2)}) copy-start(bf16[128,128]{1,0:T(8,128)(2,1)} %param.24) | copy-start | bytes 98308
  69.4 33.9 %copy-start.11 = (bf16[128,128]{1,0:T(8,128)(2,1)S(1)}, bf16[128,128]{1,0:T(8,128)(2,1)}, u32[]{:S(2)}) copy-start(bf16[128,128]{1,0:T(8,128)(2,1)} %param.26) | copy-start | bytes 98308
  69.4 34.0 %copy-start.12 = (bf16[128,128]{1,0:T(8,128)(2,1)S(1)}, bf16[128,128]{1,0:T(8,128)(2,1)}, u32[]{:S(2)}) copy-start(bf16[128,128]{1,0:T(8,128)(2,1)} %param.25) | copy-start | bytes 98308
  69.4 35.2 %copy-start.8 = (f32[128,128]{1,0:T(8,128)S(1)}, f32[128,128]{1,0:T(8,128)}, u32[]{:S(2)}) copy-start(f32[128,128]{1,0:T(8,128)} %param.27) | copy-start | bytes 196612
  69.4 35.3 %copy-start.9 = (f32[128,128]{1,0:T(8,128)S(1)}, f32[128,128]{1,0:T(8,128)}, u32[]{:S(2)}) copy-start(f32[128,128]{1,0:T(8,128)} %param.31) | copy-start | bytes 196612
  69.4 36.0 %copy-start.13 = (bf16[4,32,32]{2,1,0:T(8,128)(2,1)S(1)}, bf16[4,32,32]{2,1,0:T(8,128)(2,1)}, u32[]{:S(2)}) copy-start(bf16[4,32,32]{2,1,0:T(8,128)(2,1)} %param.28) | copy-start | bytes 24580
  69.4 36.3 %copy-start.19 = (f32[128]{0:T(128)S(1)}, f32[128]{0:T(128)}, u32[]{:S(2)}) copy-start(f32[128]{0:T(128)} %param.30) | copy-start | bytes 1540
  69.4 36.4 %copy-start.5 = (bf16[2048,128]{1,0:T(8,128)(2,1)S(1)}, bf16[2048,128]{1,0:T(8,128)(2,1)}, u32[]{:S(2)}) copy-start(bf16[2048,128]{1,0:T(8,128)(2,1)} %param.23) | copy-start | bytes 1572868
  101.0 4.8 %copy-start.1 = (bf16[128,2048]{1,0:T(8,128)(2,1)S(1)}, bf16[128,2048]{1,0:T(8,128)(2,1)}, u32[]{:S(2)}) copy-start(bf16[128,2048]{1,0:T(8,128)(2,1)} %shard_map.200) | copy-start | bytes 1572868
  107.7 21.9 %copy-start.14 = (bf16[4,32,32]{2,1,0:T(8,128)(2,1)S(1)}, bf16[4,32,32]{2,1,0:T(8,128)(2,1)}, u32[]{:S(2)}) copy-start(bf16[4,32,32]{2,1,0:T(8,128)(2,1)} %param.28) | copy-start | bytes 24580
  107.7 22.1 %copy-start.15 = (bf16[4,32,32]{2,1,0:T(8,128)(2,1)S(1)}, bf16[4,32,32]{2,1,0:T(8,128)(2,1)}, u32[]{:S(2)}) copy-start(bf16[4,32,32]{2,1,0:T(8,128)(2,1)} %param.29) | copy-start | bytes 24580
  107.9 22.9 %copy-start.6 = (f32[128,128]{0,1:T(8,128)S(1)}, f32[128,128]{0,1:T(8,128)}, u32[]{:S(2)}) copy-start(f32[128,128]{0,1:T(8,128)} %get-tuple-element.44) | copy-start | bytes 196612
  128.6 2.9 %copy-start.7 = (f32[256,128]{1,0:T(8,128)S(1)}, f32[256,128]{1,0:T(8,128)}, u32[]{:S(2)}) copy-start(f32[256,128]{1,0:T(8,128)} %get-tuple-element.93) | copy-start | bytes 393220
where the time goes:
time: 133 us; the launch traced here: 132 us
  Pallas kernels  88 us (66%)
  matrix products  29.9 us (22%)
  local copies, waits for them, and re-layouts  7.85 us (6%)
  other arithmetic  4.98 us (4%)
  between operations  1.41 us (1%)
    pallas_call x1, Pallas kernels, dispatch(): pl.pallas_call(functools.partial(dispatch_kernel, n_sp, n_tp), out_shape=...  37.7 us
    pallas_call x1, Pallas kernels, give_back(): pl.pallas_call(functools.partial(return_kernel, n_sp, n_tp), out_shape=ja...  31.6 us
    pallas_call x1, Pallas kernels, close(): pl.pallas_call(functools.partial(close_kernel, n_sp, n_tp), out_shape=(ja...  18.7 us
    unnamed x48, local copies, waits for them, and re-layouts  5.42 us
    dot_general x1, matrix products, local(): jnp.einsum('secd,edf->secf', tokens_in, w_up, preferred_element_type=jnp....  3.61 us
    dot_general x2, matrix products, to_slots(): tokens = jnp.dot(lands_any, rows_in, preferred_element_type=jnp.float32)  3.14 us
    dot_general x1, matrix products, weight_grads(): jnp.einsum('secf,secd->efd', act_low, grads_in, preferred_element_type=jn...  2.76 us

commit v1 on v0

v1 whole, which is shorter than its diff:
```python
import functools

import jax
import jax.numpy as jnp
from jax import lax
from jax.experimental import pallas as pl
from jax.experimental.pallas import tpu as pltpu
from jax.sharding import PartitionSpec as P

RATE_SCALE = 8.0
CLAMP_LIMIT = 7.0
GLU_ALPHA = 1.702
CORES = 2
MESH = pl.DeviceIdType.MESH
VMEM_LIMIT = 60 * 1024 * 1024
GELU_A = 0.7978845608028654
GELU_B = 0.044715
BF = jnp.bfloat16
F32 = jnp.float32


def aligned(value, size):
    return pl.multiple_of(value * size, size)


def part(index, size):
    return pl.ds(aligned(index, size), size)


def remote(src, dst, send_sem, recv_sem, device):
    return pltpu.make_async_remote_copy(
        src_ref=src,
        dst_ref=dst,
        send_sem=send_sem,
        recv_sem=recv_sem,
        device_id=device,
        device_id_type=MESH,
    )


def dot(a, b, da=1, db=0):
    return lax.dot_general(a, b, (((da,), (db,)), ((), ())), preferred_element_type=F32)


def minus_expm1(x):
    series = x * (1.0 + x * (0.5 + x * (1 / 6 + x * (1 / 24 + x * (1 / 120 + x * (1 / 720))))))
    return jnp.where(x > -0.25, -series, 1.0 - jnp.exp(x))


def softplus(v):
    u = jnp.exp(-jnp.abs(v))
    series = u * (1.0 - u * (0.5 - u * (1 / 3 - u * (0.25 - u * (0.2 - u * (1 / 6))))))
    return jnp.maximum(v, 0.0) + jnp.where(u < 0.06, series, jnp.log(1.0 + u))


def sigmoid(x):
    return 1.0 / (1.0 + jnp.exp(-x))


class Place:
    def __init__(self, n_sp, n_tp):
        self.n, self.nt, self.ny = n_sp, n_tp, n_tp // CORES
        self.s, self.t = lax.axis_index("sp"), lax.axis_index("tp")
        self.y, self.c = self.t // CORES, lax.rem(self.t, CORES)
        self.partner = (self.s, self.y * CORES + 1 - self.c)
        quarter = n_sp // 4
        mid = lax.rem(self.s // quarter + self.s // (2 * quarter), 2)
        self.far = (2 * quarter + quarter * mid, 2 * quarter + quarter * (1 - mid))

    def mirror(self, i):
        found, bit = 0, 1
        while bit < self.n:
            found = found + lax.rem(self.s // bit + i // bit, 2) * bit
            bit *= 2
        return found

    def y_peer(self, j):
        return lax.rem(self.y + j, self.ny)

    def y_source(self, j):
        return lax.rem(self.y + self.ny - j, self.ny)

    def tp_of(self, y, c):
        return y * CORES + c

    def q(self, j, same=True):
        return self.tp_of(self.y_source(j), self.c if same else 1 - self.c)

    def y_dev(self, j):
        return (self.s, self.tp_of(self.y_peer(j), self.c))

    def dev(self, i, j):
        return (self.mirror(i), self.tp_of(self.y_peer(j), self.c))


def fused_kernel(n, nt, head_dim, *refs):
    (
        stream, cot, ids, rw, wg_h, wu_h, wd_h, op_h, mixed, rec_in, branch, before, rgate, igate,
        dparam, dshift,
        o_gate, o_up, o_down, o_proj, o_rec, o_branch,
        wg, wu, wd, opf, sc, pos, land, land2, land_t, src, inb, msrc, mb, act, dg, du, wgp, wup,
        q, qin, qsum, ret, ag, au, gp, gin, gsum, yin, gy, xin, gx, zin, st_gate, st_up, st_down,
        level, coef, link, links, mixed_t, dm0, adj0, base,
        w_sem, s1, r1, sy, ry, sx, rx, sm, rm, smy, rmy, smx, rmx, soy, roy, sox, rox,
        sq, rq, sr, rr, sk, rk, sg, rg, sgy, rgy, sgx, rgx, sgz, rgz, o_sem,
    ) = refs
    at = Place(n, nt)
    ny = at.ny
    tok, width = cot.shape
    rows = land.shape[0] // n
    cols = width // nt
    wl, hidden = opf.shape[2], wg.shape[1]
    top = ids.shape[1]
    blk = width // n
    half = n // 2
    quarter = n // 4
    groups = [list(range(nt))] if wl % 128 == 0 else [[b] for b in range(nt)]
    ftile = min(256, hidden)

    def cat(ref, sl, group):
        parts = [ref[b, sl, :] for b in group]
        return parts[0] if len(parts) == 1 else jnp.concatenate(parts, axis=1)

    def spread(value, group, put):
        for at_b, b in enumerate(group):
            put(b, value[:, at_b * wl : (at_b + 1) * wl])

    def loop(lo, hi, body):
        def step(i, carry):
            body(i)
            return carry

        lax.fori_loop(lo, hi, step, 0)

    barrier = pltpu.get_barrier_semaphore()

    def greet(device):
        pl.semaphore_signal(barrier, inc=1, device_id=device, device_id_type=MESH)

    def greet_all(i):
        for j in range(ny):
            greet(at.dev(i, j))

    loop(1, n, greet_all)
    for j in range(1, ny):
        greet(at.y_dev(j))
    greet(at.partner)

    weights = [
        pltpu.make_async_copy(op_h, opf.at[at.t], w_sem.at[0]),
        pltpu.make_async_copy(wg_h, wg, w_sem.at[1]),
        pltpu.make_async_copy(wu_h, wu, w_sem.at[2]),
        pltpu.make_async_copy(wd_h, wd, w_sem.at[3]),
    ]
    for copy in weights:
        copy.start()

    lane = lax.broadcasted_iota(jnp.int32, (tok, tok), 1)
    sub = lax.broadcasted_iota(jnp.int32, (tok, tok), 0)
    eye = lane == sub
    eye_low = jnp.where(eye, 1.0, 0.0).astype(BF)
    tri = jnp.where(sub < lane, 1.0, 0.0).astype(BF)
    expert_at = lax.broadcasted_iota(jnp.int32, (n, tok), 0).astype(F32)
    named = []
    for k in range(top):
        column = ids[:, k : k + 1].astype(F32)
        row = jnp.sum(jnp.where(eye, column, 0.0), axis=0, keepdims=True)
        named.append(expert_at == row)
    count = functools.reduce(jnp.add, [jnp.where(m, 1.0, 0.0) for m in named])
    earlier = dot(count.astype(BF), tri)
    for k in range(top):
        pos[k] = jnp.where(named[k], earlier, -1.0)
    slot = lax.broadcasted_iota(jnp.int32, (rows, tok), 0).astype(F32)

    def lands(i):
        e = at.mirror(i)
        hits = [jnp.where(pos[k, pl.ds(e, 1), :] == slot, 1.0, 0.0) for k in range(top)]
        land[part(i, rows), :] = functools.reduce(jnp.add, hits).astype(BF)
        for k in range(top):
            land2[part(i, rows), k * tok : (k + 1) * tok] = hits[k].astype(BF)

    loop(0, n, lands)

    def scale(b):
        sl = part(b, cols)
        value = cot[:, sl].astype(F32)
        for k in range(top):
            sc[k * tok : (k + 1) * tok, sl] = (rw[:, k : k + 1] * value).astype(BF)

    loop(0, nt, scale)

    def to_slots(lo, hi, tp, put):
        sl, rs = part(tp, cols), slice(lo * rows, hi * rows)
        put(rs, slice(0, cols), dot(land[rs, :], stream[:, sl]).astype(BF))
        put(rs, slice(cols, 2 * cols), dot(land2[rs, :], sc[:, sl]).astype(BF))

    def put_src(j):
        def put(rs, cs, value):
            src[j, rs, cs] = value

        return put

    for j in range(ny):
        to_slots(1, half, at.q(j), put_src(j))

    def first(i, j):
        return remote(
            src.at[j, part(i, rows), :],
            inb.at[at.q(j), part(i, rows), :],
            s1.at[i, j],
            r1.at[i, j],
            (at.mirror(i), at.t),
        )

    def along_y(i, j, outgoing):
        spot = inb.at[at.t if outgoing else at.q(j), part(i, rows), :]
        return remote(spot, spot, sy.at[i, j], ry.at[i, j], at.y_dev(j))

    def across(i, j, outgoing):
        spot = inb.at[at.q(j, outgoing), part(i, rows), :]
        return remote(spot, spot, sx.at[i, j], rx.at[i, j], at.partner)

    def op_y(j, outgoing):
        spot = opf.at[at.t if outgoing else at.q(j)]
        return remote(spot, spot, soy.at[j], roy.at[j], at.y_dev(j))

    def op_x(j, outgoing):
        spot = opf.at[at.q(j, outgoing)]
        return remote(spot, spot, sox.at[j], rox.at[j], at.partner)

    def m_first(i):
        return remote(
            msrc.at[part(i, rows), :],
            mb.at[at.t, part(i, rows), :],
            sm.at[i],
            rm.at[i],
            (at.mirror(i), at.t),
        )

    def m_y(j, outgoing):
        spot = mb.at[at.t if outgoing else at.q(j)]
        return remote(spot, spot, smy.at[j], rmy.at[j], at.y_dev(j))

    def m_x(j, outgoing):
        spot = mb.at[at.q(j, outgoing)]
        return remote(spot, spot, smx.at[j], rmx.at[j], at.partner)

    weights[0].wait()
    pl.semaphore_wait(barrier, (n - 1) * ny + ny - 1 + 1)
    for j in range(1, ny):
        op_y(j, True).start()
    op_x(0, True).start()

    def send_near(i):
        for j in range(ny):
            first(i, j).start()

    loop(1, half, send_near)
    to_slots(half, n, at.t, put_src(0))
    msrc[...] = dot(land[...], mixed[...], 1, 1).astype(BF)

    def own_slots(tp):
        def put(rs, cs, value):
            inb[tp, rs, cs] = value

        to_slots(0, 1, tp, put)

    loop(0, nt, own_slots)
    for far in at.far:
        loop(0, quarter, lambda k: first(far + k, 0).start())
    mb[at.t, 0:rows, :] = msrc[0:rows, :]
    loop(1, half, lambda i: m_first(i).start())
    for far in at.far:
        loop(0, quarter, lambda k: m_first(far + k).start())

    lane_w = lax.broadcasted_iota(jnp.int32, (wl, wl), 1)
    sub_w = lax.broadcasted_iota(jnp.int32, (wl, wl), 0)
    eye_w = lane_w == sub_w

    def to_col(row):
        return jnp.sum(jnp.where(eye_w, row, 0.0), axis=1, keepdims=True)

    def to_row(col):
        return jnp.sum(jnp.where(eye_w, col, 0.0), axis=0, keepdims=True)

    repeat = jnp.where(
        lax.rem(lax.broadcasted_iota(jnp.int32, (head_dim, wl), 1), head_dim)
        == lax.broadcasted_iota(jnp.int32, (head_dim, wl), 0),
        1.0,
        0.0,
    ).astype(BF)
    same_head = lax.div(lane_w, head_dim) == lax.div(sub_w, head_dim)

    def diagonal(ref):
        return jnp.where(same_head, dot(ref[...], repeat), 0.0).astype(BF)

    time_at = lax.broadcasted_iota(jnp.int32, (wl, tok), 1)
    rec = rec_in[...]
    rec_gate = sigmoid(dot(diagonal(rgate), rec, 0, 0))
    in_gate = sigmoid(dot(diagonal(igate), rec, 0, 0))
    rec = rec.astype(F32)
    soft = to_col(softplus(-dparam[...]))
    log_decay = -RATE_SCALE * rec_gate * soft + dshift[...]
    decay = jnp.exp(log_decay)
    at_start = (time_at == 0) & (at.s == 0)
    raw_mult = jnp.sqrt(minus_expm1(2.0 * log_decay))
    multiplier = jnp.where(at_start, 1.0, raw_mult)
    old = before[...]
    state = decay * old + multiplier * in_gate * rec
    x = branch[...].astype(F32)
    th = jnp.tanh(GELU_A * (x + GELU_B * x * x * x))
    gelu = 0.5 * x * (1.0 + th)
    slope = 0.5 * (1.0 + th) + 0.5 * x * (1.0 - th * th) * GELU_A * (1.0 + 3.0 * GELU_B * x * x)
    mult_part = jnp.where(at_start, 0.0, in_gate * rec * decay * decay / raw_mult)
    coef[0] = gelu
    coef[1] = state * slope
    coef[2] = (old * decay - mult_part) * (-RATE_SCALE * soft) * rec_gate * (1.0 - rec_gate)
    coef[3] = multiplier * rec * in_gate * (1.0 - in_gate)
    coef[4] = multiplier * in_gate
    step_decay = jnp.where(time_at == tok - 1, 0.0, pltpu.roll(decay, tok - 1, 1))
    tail = jnp.where(time_at == tok - 1, 1.0, pltpu.roll(decay, tok - 1, 1))
    shift, depth = 1, 0
    while shift < tok:
        level[depth] = step_decay
        step_decay = step_decay * pltpu.roll(step_decay, tok - shift, 1)
        tail = tail * jnp.where(time_at < tok - shift, pltpu.roll(tail, tok - shift, 1), 1.0)
        shift, depth = shift * 2, depth + 1
    coef[5] = tail
    coef[6] = decay
    link[...] = jnp.zeros(link.shape, F32)
    link[0:1, :] = to_row(decay[:, 0:1] * tail[:, 0:1])
    dm0[...] = dot(cot[...], opf[at.t])
    mixed_t[...] = dot(eye_low, mixed[...], 1, 1).astype(BF)
    land_t[...] = dot(eye_low, land[...], 1, 1).astype(BF)

    def own_part(b):
        base[part(b, cols), :] = dot(cot[:, part(b, cols)], mixed_t[...], 0, 0)

    loop(0, nt, own_part)
    for copy in weights[1:]:
        copy.wait()

    def near_in(i):
        for j in range(ny):
            first(i, j).wait_recv()
            across(i, j, True).start()

    def far_in(i):
        first(i, 0).wait_recv()
        for j in range(1, ny):
            along_y(i, j, True).start()
        across(i, 0, True).start()

    def far_pass(i):
        for j in range(1, ny):
            along_y(i, j, False).wait_recv()
            across(i, j, True).start()

    def all_here(i):
        for j in range(ny):
            across(i, j, False).wait_recv()

    def forward(r0, size):
        rs = pl.ds(r0, size)

        def tile(f):
            fs = part(f, ftile)
            gate = up = d_act = 0.0
            for b in range(nt):
                bs = slice(b * cols, (b + 1) * cols)
                tokens, grads = inb[b, rs, 0:cols], inb[b, rs, cols : 2 * cols]
                gate = gate + dot(tokens, wg[bs, fs])
                up = up + dot(tokens, wu[bs, fs])
                d_act = d_act + dot(grads, wd[fs, bs], 1, 1)
            glu = jnp.minimum(gate, CLAMP_LIMIT)
            lin = jnp.clip(up, -CLAMP_LIMIT, CLAMP_LIMIT) + 1.0
            sig = sigmoid(GLU_ALPHA * glu)
            gs = glu * sig
            act[rs, fs] = (gs * lin).astype(BF)
            curve = lin * (sig + GLU_ALPHA * gs * (1.0 - sig))
            dg[rs, fs] = jnp.where(gate > CLAMP_LIMIT, 0.0, d_act * curve).astype(BF)
            du[rs, fs] = jnp.where(jnp.abs(up) > CLAMP_LIMIT, 0.0, d_act * gs).astype(BF)

        loop(0, hidden // ftile, tile)

    def project(r0, size):
        rs = pl.ds(r0, size)
        for group in groups:
            value = dot(dg[rs, :], cat(wgp, slice(None), group))
            value = value + dot(du[rs, :], cat(wup, slice(None), group))

            def put(b, piece):
                q[b, rs, :] = piece.astype(BF)

            spread(value, group, put)

    def q_core(g, r0, size, j, outgoing):
        yj = at.y_peer(j)
        return remote(
            q.at[at.tp_of(yj, 1 - at.c), pl.ds(r0, size), :],
            qin.at[j, pl.ds(r0, size), :],
            sq.at[g, j],
            rq.at[g, j],
            at.partner,
        )

    def ret_copy(i, j):
        return remote(
            qsum.at[j, part(i, rows), :],
            ret.at[j, part(i, rows), :],
            sr.at[i, j],
            rr.at[i, j],
            at.dev(i, j),
        )

    def q_send(g, r0, size):
        for j in range(ny):
            q_core(g, r0, size, j, True).start()

    def q_reduce(g, r0, size):
        rs = pl.ds(r0, size)
        for j in range(ny):
            q_core(g, r0, size, j, False).wait_recv()
            mine = q[at.tp_of(at.y_peer(j), at.c), rs, :].astype(F32)
            qsum[j, rs, :] = (mine + qin[j, rs, :].astype(F32)).astype(BF)

    def ret_send(i):
        for j in range(ny):
            ret_copy(i, j).start()

    loop(1, half, near_in)
    for far in at.far[:1]:
        loop(0, quarter, lambda k: far_in(far + k))
    for j in range(1, ny):
        op_y(j, False).wait_recv()
        op_x(j, True).start()
    for far in at.far[:1]:
        loop(0, quarter, lambda k: far_pass(far + k))
    for j in range(ny):
        op_x(j, False).wait_recv()

    def weight_maps(f):
        fs = part(f, ftile)
        for group in groups:
            for ref, out in ((wg, wgp), (wu, wup)):
                value = 0.0
                for b in range(nt):
                    bs = slice(b * cols, (b + 1) * cols)
                    value = value + dot(ref[bs, fs], cat(opf, bs, group), 0, 0)

                def put(b, piece):
                    out[b, fs, :] = piece.astype(BF)

                spread(value, group, put)

    loop(0, hidden // ftile, weight_maps)
    loop(1, half, all_here)
    near_rows = half * rows
    far_rows = quarter * rows
    forward(0, near_rows)
    project(0, near_rows)
    q_send(0, 0, near_rows)
    far_a, far_b = (aligned(far, rows) for far in at.far)
    loop(0, quarter, lambda k: all_here(at.far[0] + k))
    forward(far_a, far_rows)
    project(far_a, far_rows)
    q_send(1, far_a, far_rows)
    q_reduce(0, 0, near_rows)
    loop(0, quarter, lambda k: far_in(at.far[1] + k))
    loop(0, quarter, lambda k: far_pass(at.far[1] + k))
    q_reduce(1, far_a, far_rows)
    loop(0, quarter, lambda k: all_here(at.far[1] + k))
    forward(far_b, far_rows)
    project(far_b, far_rows)
    q_send(2, far_b, far_rows)

    ret[0, 0:rows, :] = qsum[0, 0:rows, :]
    for j in range(1, ny):
        ret_copy(0, j).start()
    loop(1, half, ret_send)
    loop(0, quarter, lambda k: ret_send(at.far[0] + k))

    loop(1, n, lambda i: m_first(i).wait_recv())
    for j in range(1, ny):
        m_y(j, True).start()
    m_x(0, True).start()

    q_reduce(2, far_b, far_rows)
    loop(0, quarter, lambda k: ret_send(at.far[1] + k))

    for j in range(1, ny):
        m_y(j, False).wait_recv()
        m_x(j, True).start()
    for j in range(ny):
        m_x(j, False).wait_recv()

    def inner(f):
        fs = part(f, ftile)
        for group in groups:
            right = cat(mb, slice(None), group)
            for ref, out in ((dg, ag), (du, au)):
                value = dot(ref[:, fs], right, 0, 0)

                def put(b, piece):
                    out[b, fs, :] = piece.astype(BF)

                spread(value, group, put)

    loop(0, hidden // ftile, inner)

    def g_core(k, j):
        return remote(
            gp.at[k, at.tp_of(at.y_peer(j), 1 - at.c)],
            gin.at[k, j],
            sg.at[k, j],
            rg.at[k, j],
            at.partner,
        )

    def outer(k):
        ds = part(at.mirror(k), blk)
        own = base[ds, :]
        for group in groups:
            value = dot(wg[ds, :], cat(ag, slice(None), group))
            value = value + dot(wu[ds, :], cat(au, slice(None), group))

            def put(b, piece):
                gp[k, b] = (piece + jnp.where(at.t == b, own, 0.0)).astype(BF)

            spread(value, group, put)
        for j in range(ny):
            g_core(k, j).start()

    def g_y(k, j):
        return remote(gsum.at[k, j], yin.at[k, j], sgy.at[k, j], rgy.at[k, j], at.y_dev(j))

    def g_x(k):
        return remote(gy.at[k], xin.at[k], sgx.at[k], rgx.at[k], (at.mirror(1), at.t))

    def g_z(k):
        return remote(gx.at[k], zin.at[k], sgz.at[k], rgz.at[k], (at.mirror(2 * k), at.t))

    def core_step(k):
        for j in range(ny):
            g_core(k, j).wait_recv()
            mine = gp[k, at.tp_of(at.y_peer(j), at.c)].astype(F32)
            gsum[k, j] = (mine + gin[k, j].astype(F32)).astype(BF)
            if j:
                g_y(k, j).start()

    def y_step(k):
        total = gsum[k, 0].astype(F32)
        for j in range(1, ny):
            g_y(k, j).wait_recv()
            total = total + yin[k, j].astype(F32)
        gy[k] = total.astype(BF)

    def down(i):
        return n - 1 - i

    loop(0, n, lambda i: outer(down(i)))
    loop(0, n, lambda i: core_step(down(i)))

    def wide_tile(d):
        per = cols // min(256, cols)
        size = cols // per
        b, inside = lax.div(d, per), lax.rem(d, per)
        tokens = inb[b, :, part(inside, size)]
        out = part(d, size)
        st_gate[out, :] = dot(tokens, dg[...], 0, 0).astype(BF)
        st_up[out, :] = dot(tokens, du[...], 0, 0).astype(BF)

    loop(0, width // min(256, cols), wide_tile)
    outs = [
        pltpu.make_async_copy(st_gate, o_gate, o_sem.at[0]),
        pltpu.make_async_copy(st_up, o_up, o_sem.at[1]),
        pltpu.make_async_copy(st_down, o_down, o_sem.at[2]),
    ]
    outs[0].start()
    outs[1].start()

    def ret_here(i):
        for j in range(ny):
            ret_copy(i, j).wait_recv()

    for j in range(1, ny):
        ret_copy(0, j).wait_recv()
    loop(1, n, ret_here)
    total = dm0[...]
    for j in range(ny):
        total = total + dot(land_t[...], ret[j])
    d_mixed = total.T
    o_branch[...] = d_mixed * coef[1]
    run = d_mixed * coef[0]
    shift = 1
    for k in range(depth):
        run = run + level[k] * pltpu.roll(run, tok - shift, 1)
        shift *= 2
    adj0[...] = run
    link[1:2, :] = to_row(coef[6][:, 0:1] * run[:, 0:1])

    def link_copy(i):
        return remote(link, links.at[i], sk.at[i], rk.at[i], (at.mirror(i), at.t))

    loop(1, n, lambda i: link_copy(i).start())

    loop(0, n, lambda i: y_step(down(i)))
    loop(0, half, lambda k: g_x(2 * (half - 1 - k) + 1).start())

    def down_tile(f):
        fs = part(f, ftile)
        left = act[:, fs]
        for b in range(nt):
            bs = slice(b * cols, (b + 1) * cols)
            st_down[fs, bs] = dot(left, inb[b, :, cols : 2 * cols], 0, 0).astype(BF)

    loop(0, hidden // ftile, down_tile)
    outs[2].start()

    loop(1, n, lambda i: link_copy(i).wait_recv())
    links[0] = link[...]

    def compose(k, carry):
        p = n - 1 - k
        lower = links[at.mirror(p)]
        return jnp.where(p > at.s, lower[0:1] * carry + lower[1:2], carry)

    carried = lax.fori_loop(0, n, compose, jnp.zeros((1, wl), F32))
    adjoint = adj0[...] + coef[5] * to_col(carried)
    d_rec = (adjoint * coef[2]).astype(BF)
    d_in = (adjoint * coef[3]).astype(BF)
    o_rec[...] = adjoint * coef[4] + dot(diagonal(rgate), d_rec) + dot(diagonal(igate), d_in)

    def x_step(i):
        k = half - 1 - i
        g_x(2 * k + 1).wait_recv()
        gx[k] = (gy[2 * k].astype(F32) + xin[2 * k + 1].astype(F32)).astype(BF)

    loop(0, half, x_step)
    loop(0, half - 1, lambda i: g_z(half - 1 - i).start())
    o_proj[...] = gx[0].astype(F32)

    def z_step(i):
        k = i + 1
        g_z(k).wait_recv()
        o_proj[...] += zin[k].astype(F32)

    loop(0, half - 1, z_step)

    def drain(i):
        link_copy(i).wait_send()
        m_first(i).wait_send()
        first(i, 0).wait_send()
        across(i, 0, True).wait_send()
        for j in range(1, ny):
            across(i, j, True).wait_send()

            @pl.when(i < half)
            def _():
                first(i, j).wait_send()

            @pl.when(i >= half)
            def _():
                along_y(i, j, True).wait_send()

        for j in range(ny):
            ret_copy(i, j).wait_send()

    loop(1, n, drain)
    for j in range(1, ny):
        ret_copy(0, j).wait_send()
        op_y(j, True).wait_send()
        m_y(j, True).wait_send()
    for j in range(ny):
        op_x(j, True).wait_send()
        m_x(j, True).wait_send()
        q_core(0, 0, near_rows, j, True).wait_send()
        q_core(1, far_a, far_rows, j, True).wait_send()
        q_core(2, far_b, far_rows, j, True).wait_send()

    def drain_sums(k):
        for j in range(ny):
            g_core(k, j).wait_send()
            if j:
                g_y(k, j).wait_send()

    loop(0, n, drain_sums)
    loop(0, half, lambda k: g_x(2 * k + 1).wait_send())
    loop(1, half, lambda k: g_z(k).wait_send())
    for copy in outs:
        copy.wait()


def fused(args, n, nt):
    (stream, cot, ids, rw, wg, wu, wd, op, mixed, rec_in, branch, before, rgate, igate, dparam, dshift) = args
    tok, width = cot.shape
    top = ids.shape[1]
    local_experts, _, hidden = wg.shape
    assert local_experts == 1
    rows = 2 * tok * top // n
    total, ny, cols, wl, blk, half = n * rows, nt // CORES, width // nt, op.shape[1], width // n, n // 2
    head_dim = rgate.shape[1]
    channels = wl
    dma = pltpu.SemaphoreType.DMA

    def buf(*shape, dtype=BF):
        return pltpu.VMEM(shape, dtype)

    depth = max(1, (tok - 1).bit_length())
    scratch = [
        buf(width, hidden), buf(width, hidden), buf(hidden, width),
        buf(nt, width, wl),
        buf(top * tok, width),
        buf(top, n, tok, dtype=F32),
        buf(total, tok), buf(total, top * tok), buf(tok, total),
        buf(ny, total, 2 * cols), buf(nt, total, 2 * cols),
        buf(total, wl), buf(nt, total, wl),
        buf(total, hidden), buf(total, hidden), buf(total, hidden),
        buf(nt, hidden, wl), buf(nt, hidden, wl),
        buf(nt, total, wl), buf(ny, total, wl), buf(ny, total, wl), buf(ny, total, wl),
        buf(nt, hidden, wl), buf(nt, hidden, wl),
        buf(n, nt, blk, wl), buf(n, ny, blk, wl), buf(n, ny, blk, wl), buf(n, ny, blk, wl),
        buf(n, blk, wl), buf(n, blk, wl), buf(half, blk, wl), buf(half, blk, wl),
        buf(width, hidden), buf(width, hidden), buf(hidden, width),
        buf(depth, wl, tok, dtype=F32), buf(7, wl, tok, dtype=F32),
        buf(8, wl, dtype=F32), buf(n, 8, wl, dtype=F32),
        buf(tok, wl), buf(tok, wl, dtype=F32), buf(wl, tok, dtype=F32), buf(width, wl, dtype=F32),
        dma((4,)),
        dma((n, ny)), dma((n, ny)), dma((n, ny)), dma((n, ny)), dma((n, ny)), dma((n, ny)),
        dma((n,)), dma((n,)), dma((ny,)), dma((ny,)), dma((ny,)), dma((ny,)),
        dma((ny,)), dma((ny,)), dma((ny,)), dma((ny,)),
        dma((3, ny)), dma((3, ny)), dma((n, ny)), dma((n, ny)), dma((n,)), dma((n,)),
        dma((n, ny)), dma((n, ny)), dma((n, ny)), dma((n, ny)),
        dma((n,)), dma((n,)), dma((half,)), dma((half,)), dma((3,)),
    ]
    vm = pl.BlockSpec(memory_space=pltpu.VMEM)
    hb = pl.BlockSpec(memory_space=pl.ANY)
    shape = jax.ShapeDtypeStruct
    return pl.pallas_call(
        functools.partial(fused_kernel, n, nt, head_dim),
        out_shape=(
            shape((width, hidden), BF),
            shape((width, hidden), BF),
            shape((hidden, width), BF),
            shape((blk, wl), F32),
            shape((channels, tok), F32),
            shape((channels, tok), F32),
        ),
        in_specs=[vm] * 4 + [hb] * 4 + [vm] * 8,
        out_specs=[hb] * 3 + [vm] * 3,
        scratch_shapes=scratch,
        compiler_params=pltpu.CompilerParams(
            collective_id=0, has_side_effects=True, vmem_limit_bytes=VMEM_LIMIT
        ),
    )(
        stream, cot, ids, rw, wg[0], wu[0], wd[0], op, mixed, rec_in, branch, before,
        rgate.reshape(-1, head_dim), igate.reshape(-1, head_dim), dparam[None], dshift,
    )


def local(*args):
    n, nt = lax.axis_size("sp"), lax.axis_size("tp")
    gate, up, down, proj, rec, branch = fused(args, n, nt)
    return gate[None], up[None], down[None], proj, rec, branch


def solution(mesh):
    placed = (
        P("sp", None),
        P("sp", None),
        P("sp", None),
        P("sp", None),
        P("sp", None, "tp"),
        P("sp", None, "tp"),
        P("sp", "tp", None),
        P(None, "tp"),
        P("tp", "sp"),
        P("tp", "sp"),
        P("tp", "sp"),
        P("tp", "sp"),
        P("tp", None, None),
        P("tp", None, None),
        P("tp"),
        P("tp", "sp"),
    )
    return jax.shard_map(
        local,
        mesh=mesh,
        in_specs=placed,
        out_specs=(
            P("sp", None, "tp"),
            P("sp", None, "tp"),
            P("sp", "tp", None),
            P("sp", "tp"),
            P("tp", "sp"),
            P("tp", "sp"),
        ),
        check_vma=False,
    )
```

time: 133 us -> 109 us (0.82)
  matrix products: 29.9 us -> 0 us
  Pallas kernels: 88 us -> 96.3 us
  other arithmetic: 4.98 us -> 0 us
  local copies, waits for them, and re-layouts: 7.85 us -> 11.6 us
    dot_general x18 -> x0, matrix products: 29.9 us -> none  [the longest x1 3.61 us: local(): jnp.einsum('secd,edf->secf', tokens_in, w_up, preferred_element_type=jnp....]
    pallas_call x3 -> x1, Pallas kernels: 88 us -> 96.3 us  [fused(): pl.pallas_call(functools.partial(fused_kernel, n, nt, head_dim), out_shap...]
    unnamed x48 -> x18, local copies, waits for them, and re-layouts: 5.42 us -> 11.6 us
    convert_element_type x4 -> x0, other arithmetic: 2.74 us -> none  [the longest x2 1.23 us: to_slots(): (route_weights[:, k:k + 1] * cot_in.astype(jnp.float32)).astype(jnp.bfloa...]
where the time goes in v1:
time: 109 us
  Pallas kernels  96.3 us (88%)
  local copies, waits for them, and re-layouts  11.6 us (11%)
    pallas_call x1, Pallas kernels, fused(): pl.pallas_call(functools.partial(fused_kernel, n, nt, head_dim), out_shap...  96.3 us
    unnamed x18, local copies, waits for them, and re-layouts  11.6 us

profile of v1, /device:TPU:0, one launch (start us, length us, event | category | flops | bytes accessed | tf_op | source)
XLA Modules:
  0.0 108.6 jit_solution(11639486072040274376)
XLA Ops:
  0.6 1.4 %copy.22.refs_2_ = s32[128,2]{1,0:T(8,128)} copy(s32[128,2]{0,1:T(2,128)} %param.18) | data formatting | bytes 2048 | tf_op args[2]
  2.0 1.4 %copy.23.refs_3_ = f32[128,2]{1,0:T(8,128)} copy(f32[128,2]{0,1:T(2,128)} %param.19) | data formatting | bytes 2048 | tf_op args[3]
  3.5 96.3 %shard_map.199 = (bf16[2048,512]{1,0:T(8,128)(2,1)}, bf16[2048,512]{1,0:T(8,128)(2,1)}, bf16[512,2048]{1,0:T(8,128)(2,1)}, f32[256,128]{1,0:T(8,128)}, f32[128,128]{1,0:T(8,128)}, /*index=5*/f32[128,128]{1,0:T(8,128)}) custom-call(bf16[128,2048]{1,0:T(8,128)(2,1)} %refs_0_.1, bf16[128,2048]{1,0:T(8,128)(2,1)} %refs_1_.1, s32[128,2]{1,0:T(8,128)} %copy.22.refs_2_, ...), custom_call_target="tpu_custom_call" | custom-call | tf_op jit(solution)/shard_map/pallas_call | solution.py:739
  99.8 0.0 copy-start.1
  99.8 3.2 %copy.30 = bf16[1,2048,512]{2,1,0:T(8,128)(2,1)} copy(bf16[1,2048,512]{2,1,0:T(8,128)(2,1)} %bitcast.11) | data formatting | bytes 4194304
  103.0 0.0 copy-done.1
  103.0 0.0 copy-start
  103.0 1.3 %copy.31 = bf16[1,2048,512]{2,1,0:T(8,128)(2,1)} copy(bf16[1,2048,512]{2,1,0:T(8,128)(2,1)S(1)} %bitcast.10) | data formatting | bytes 4194304
  104.3 1.0 copy-done
  105.3 0.0 copy-start.2
  105.3 0.0 copy-start.4
  105.3 0.0 copy-start.3
  105.3 1.3 %copy.32 = bf16[1,512,2048]{2,1,0:T(8,128)(2,1)} copy(bf16[1,512,2048]{2,1,0:T(8,128)(2,1)S(1)} %bitcast.9) | data formatting | bytes 4194304
  106.6 0.0 copy-done.2
  106.7 0.7 copy.33
  107.3 0.0 copy-done.4
  107.3 0.6 copy.34
  107.9 0.0 copy-done.3
  107.9 0.6 copy.35
Async XLA Ops:
  99.8 3.2 %copy-start.1 = (bf16[2048,512]{1,0:T(8,128)(2,1)S(1)}, bf16[2048,512]{1,0:T(8,128)(2,1)}, u32[]{:S(2)}) copy-start(bf16[2048,512]{1,0:T(8,128)(2,1)} %get-tuple-element.13) | copy-start | bytes 6291460
  103.0 2.3 %copy-start = (bf16[512,2048]{1,0:T(8,128)(2,1)S(1)}, bf16[512,2048]{1,0:T(8,128)(2,1)}, u32[]{:S(2)}) copy-start(bf16[512,2048]{1,0:T(8,128)(2,1)} %get-tuple-element.14) | copy-start | bytes 6291460
  105.3 1.3 %copy-start.2 = (f32[256,128]{1,0:T(8,128)S(1)}, f32[256,128]{1,0:T(8,128)}, u32[]{:S(2)}) copy-start(f32[256,128]{1,0:T(8,128)} %get-tuple-element.27) | copy-start | bytes 393220
  105.3 2.0 %copy-start.4 = (f32[128,128]{1,0:T(8,128)S(1)}, f32[128,128]{1,0:T(8,128)}, u32[]{:S(2)}) copy-start(f32[128,128]{1,0:T(8,128)} %get-tuple-element.28) | copy-start | bytes 196612
  105.3 2.6 %copy-start.3 = (f32[128,128]{1,0:T(8,128)S(1)}, f32[128,128]{1,0:T(8,128)}, u32[]{:S(2)}) copy-start(f32[128,128]{1,0:T(8,128)} %get-tuple-element.29) | copy-start | bytes 196612

commit v2 on v1

--- a/solution.py
+++ b/solution.py
@@ -12,7 +12,7 @@
 GLU_ALPHA = 1.702
 CORES = 2
 MESH = pl.DeviceIdType.MESH
-VMEM_LIMIT = 60 * 1024 * 1024
+MIB = 1024 * 1024
 GELU_A = 0.7978845608028654
 GELU_B = 0.044715
 BF = jnp.bfloat16
@@ -64,8 +64,7 @@
         self.y, self.c = self.t // CORES, lax.rem(self.t, CORES)
         self.partner = (self.s, self.y * CORES + 1 - self.c)
         quarter = n_sp // 4
-        mid = lax.rem(self.s // quarter + self.s // (2 * quarter), 2)
-        self.far = (2 * quarter + quarter * mid, 2 * quarter + quarter * (1 - mid))
+        self.far = (2 * quarter, 3 * quarter)
 
     def mirror(self, i):
         found, bit = 0, 1
@@ -95,22 +94,23 @@
 
 def fused_kernel(n, nt, head_dim, *refs):
     (
-        stream, cot, ids, rw, wg_h, wu_h, wd_h, op_h, mixed, rec_in, branch, before, rgate, igate,
-        dparam, dshift,
-        o_gate, o_up, o_down, o_proj, o_rec, o_branch,
+        stream_h, cot_h, ids_h, rw_h, wg_h, wu_h, wd_h, op_h, mixed_h, rec_h, branch_h, before_h,
+        rgate_h, igate_h, dparam_h, dshift_h,
+        st_gate, st_up, st_down, o_proj, o_rec, o_branch,
         wg, wu, wd, opf, sc, pos, land, land2, land_t, src, inb, msrc, mb, act, dg, du, wgp, wup,
-        q, qin, qsum, ret, ag, au, gp, gin, gsum, yin, gy, xin, gx, zin, st_gate, st_up, st_down,
+        q, qin, qsum, ret, ag, au, gp, gin, gsum, yin, gy, xin, gx, zin, xin2, mx, yin2,
         level, coef, link, links, mixed_t, dm0, adj0, base,
+        stream, cot, ids, rw, mixed, rec_in, branch, before, rgate, igate, dparam, dshift,
         w_sem, s1, r1, sy, ry, sx, rx, sm, rm, smy, rmy, smx, rmx, soy, roy, sox, rox,
-        sq, rq, sr, rr, sk, rk, sg, rg, sgy, rgy, sgx, rgx, sgz, rgz, o_sem,
+        sq, rq, sr, rr, sk, rk, sg, rg, sgy, rgy, sgx, rgx, sgz, rgz, sx2, rx2, sy2, ry2,
     ) = refs
     at = Place(n, nt)
     ny = at.ny
-    tok, width = cot.shape
+    tok, width = cot_h.shape
     rows = land.shape[0] // n
     cols = width // nt
     wl, hidden = opf.shape[2], wg.shape[1]
-    top = ids.shape[1]
+    top = ids_h.shape[0]
     blk = width // n
     half = n // 2
     quarter = n // 4
@@ -132,6 +132,17 @@
 
         lax.fori_loop(lo, hi, step, 0)
 
+    pairs = (
+        (ids_h, ids), (rw_h, rw), (stream_h, stream), (cot_h, cot), (op_h, opf.at[at.t]),
+        (mixed_h, mixed), (rec_h, rec_in), (branch_h, branch), (before_h, before),
+        (rgate_h, rgate), (igate_h, igate), (dparam_h, dparam), (dshift_h, dshift),
+        (wg_h, wg), (wu_h, wu), (wd_h, wd),
+    )
+    loads = [pltpu.make_async_copy(a, b, w_sem.at[i]) for i, (a, b) in enumerate(pairs)]
+
+    for copy in loads:
+        copy.start()
+
     barrier = pltpu.get_barrier_semaphore()
 
     def greet(device):
@@ -146,14 +157,6 @@
         greet(at.y_dev(j))
     greet(at.partner)
 
-    weights = [
-        pltpu.make_async_copy(op_h, opf.at[at.t], w_sem.at[0]),
-        pltpu.make_async_copy(wg_h, wg, w_sem.at[1]),
-        pltpu.make_async_copy(wu_h, wu, w_sem.at[2]),
-        pltpu.make_async_copy(wd_h, wd, w_sem.at[3]),
-    ]
-    for copy in weights:
-        copy.start()
 
     lane = lax.broadcasted_iota(jnp.int32, (tok, tok), 1)
     sub = lax.broadcasted_iota(jnp.int32, (tok, tok), 0)
@@ -162,10 +165,10 @@
     tri = jnp.where(sub < lane, 1.0, 0.0).astype(BF)
     expert_at = lax.broadcasted_iota(jnp.int32, (n, tok), 0).astype(F32)
     named = []
+    loads[0].wait()
+    loads[1].wait()
     for k in range(top):
-        column = ids[:, k : k + 1].astype(F32)
-        row = jnp.sum(jnp.where(eye, column, 0.0), axis=0, keepdims=True)
-        named.append(expert_at == row)
+        named.append(expert_at == ids[k : k + 1, :].astype(F32))
     count = functools.reduce(jnp.add, [jnp.where(m, 1.0, 0.0) for m in named])
     earlier = dot(count.astype(BF), tri)
     for k in range(top):
@@ -181,12 +184,18 @@
 
     loop(0, n, lands)
 
+    share = [
+        jnp.sum(jnp.where(eye, rw[k : k + 1, :], 0.0), axis=1, keepdims=True) for k in range(top)
+    ]
+
     def scale(b):
         sl = part(b, cols)
         value = cot[:, sl].astype(F32)
         for k in range(top):
-            sc[k * tok : (k + 1) * tok, sl] = (rw[:, k : k + 1] * value).astype(BF)
-
+            sc[k * tok : (k + 1) * tok, sl] = (share[k] * value).astype(BF)
+
+    loads[2].wait()
+    loads[3].wait()
     loop(0, nt, scale)
 
     def to_slots(lo, hi, tp, put):
@@ -245,7 +254,8 @@
         spot = mb.at[at.q(j, outgoing)]
         return remote(spot, spot, smx.at[j], rmx.at[j], at.partner)
 
-    weights[0].wait()
+    loads[4].wait()
+    loads[5].wait()
     pl.semaphore_wait(barrier, (n - 1) * ny + ny - 1 + 1)
     for j in range(1, ny):
         op_y(j, True).start()
@@ -255,7 +265,8 @@
         for j in range(ny):
             first(i, j).start()
 
-    loop(1, half, send_near)
+    split = half - half // 4
+    loop(1, split, send_near)
     to_slots(half, n, at.t, put_src(0))
     msrc[...] = dot(land[...], mixed[...], 1, 1).astype(BF)
 
@@ -266,12 +277,9 @@
         to_slots(0, 1, tp, put)
 
     loop(0, nt, own_slots)
-    for far in at.far:
-        loop(0, quarter, lambda k: first(far + k, 0).start())
+    far_1, far_2 = at.far
+    loop(far_1, far_2, lambda i: first(i, 0).start())
     mb[at.t, 0:rows, :] = msrc[0:rows, :]
-    loop(1, half, lambda i: m_first(i).start())
-    for far in at.far:
-        loop(0, quarter, lambda k: m_first(far + k).start())
 
     lane_w = lax.broadcasted_iota(jnp.int32, (wl, wl), 1)
     sub_w = lax.broadcasted_iota(jnp.int32, (wl, wl), 0)
@@ -294,6 +302,8 @@
     def diagonal(ref):
         return jnp.where(same_head, dot(ref[...], repeat), 0.0).astype(BF)
 
+    for copy in loads[6:13]:
+        copy.wait()
     time_at = lax.broadcasted_iota(jnp.int32, (wl, tok), 1)
     rec = rec_in[...]
     rec_gate = sigmoid(dot(diagonal(rgate), rec, 0, 0))
@@ -337,7 +347,7 @@
         base[part(b, cols), :] = dot(cot[:, part(b, cols)], mixed_t[...], 0, 0)
 
     loop(0, nt, own_part)
-    for copy in weights[1:]:
+    for copy in loads[13:]:
         copy.wait()
 
     def near_in(i):
@@ -428,17 +438,6 @@
         for j in range(ny):
             ret_copy(i, j).start()
 
-    loop(1, half, near_in)
-    for far in at.far[:1]:
-        loop(0, quarter, lambda k: far_in(far + k))
-    for j in range(1, ny):
-        op_y(j, False).wait_recv()
-        op_x(j, True).start()
-    for far in at.far[:1]:
-        loop(0, quarter, lambda k: far_pass(far + k))
-    for j in range(ny):
-        op_x(j, False).wait_recv()
-
     def weight_maps(f):
         fs = part(f, ftile)
         for group in groups:
@@ -453,44 +452,53 @@
 
                 spread(value, group, put)
 
-    loop(0, hidden // ftile, weight_maps)
-    loop(1, half, all_here)
     near_rows = half * rows
     far_rows = quarter * rows
+    far_a, far_b = far_1 * rows, far_2 * rows
+    near_in(1)
+    loop(far_1, far_2, lambda i: first(i, 0).wait_send())
+    loop(split, half, send_near)
+    loop(far_2, n, lambda i: first(i, 0).start())
+    loop(1, n, lambda i: m_first(i).start())
+    loop(2, split, near_in)
+    for j in range(1, ny):
+        op_y(j, False).wait_recv()
+        op_x(j, True).start()
+    loop(far_1, far_2, far_in)
+    for j in range(ny):
+        op_x(j, False).wait_recv()
+    loop(0, hidden // ftile, weight_maps)
+    loop(far_1, far_2, far_pass)
+    loop(split, half, near_in)
+    loop(far_2, n, far_in)
+    loop(1, half, all_here)
     forward(0, near_rows)
     project(0, near_rows)
     q_send(0, 0, near_rows)
-    far_a, far_b = (aligned(far, rows) for far in at.far)
-    loop(0, quarter, lambda k: all_here(at.far[0] + k))
-    forward(far_a, far_rows)
-    project(far_a, far_rows)
-    q_send(1, far_a, far_rows)
-    q_reduce(0, 0, near_rows)
-    loop(0, quarter, lambda k: far_in(at.far[1] + k))
-    loop(0, quarter, lambda k: far_pass(at.far[1] + k))
-    q_reduce(1, far_a, far_rows)
-    loop(0, quarter, lambda k: all_here(at.far[1] + k))
-    forward(far_b, far_rows)
-    project(far_b, far_rows)
-    q_send(2, far_b, far_rows)
-
-    ret[0, 0:rows, :] = qsum[0, 0:rows, :]
-    for j in range(1, ny):
-        ret_copy(0, j).start()
-    loop(1, half, ret_send)
-    loop(0, quarter, lambda k: ret_send(at.far[0] + k))
-
     loop(1, n, lambda i: m_first(i).wait_recv())
     for j in range(1, ny):
         m_y(j, True).start()
     m_x(0, True).start()
-
-    q_reduce(2, far_b, far_rows)
-    loop(0, quarter, lambda k: ret_send(at.far[1] + k))
-
+    loop(far_1, far_2, all_here)
+    forward(far_a, far_rows)
+    project(far_a, far_rows)
+    q_send(1, far_a, far_rows)
+    loop(far_2, n, far_pass)
+    q_reduce(0, 0, near_rows)
+    q_reduce(1, far_a, far_rows)
+    ret[0, 0:rows, :] = qsum[0, 0:rows, :]
+    for j in range(1, ny):
+        ret_copy(0, j).start()
+    loop(1, far_2, ret_send)
+    loop(far_2, n, all_here)
+    forward(far_b, far_rows)
+    project(far_b, far_rows)
+    q_send(2, far_b, far_rows)
     for j in range(1, ny):
         m_y(j, False).wait_recv()
         m_x(j, True).start()
+    q_reduce(2, far_b, far_rows)
+    loop(far_2, n, ret_send)
     for j in range(ny):
         m_x(j, False).wait_recv()
 
@@ -540,13 +548,29 @@
     def g_z(k):
         return remote(gx.at[k], zin.at[k], sgz.at[k], rgz.at[k], (at.mirror(2 * k), at.t))
 
-    def core_step(k):
+    def g_x2(k, j):
+        return remote(
+            gsum.at[2 * k + 1, j], xin2.at[k, j], sx2.at[k, j], rx2.at[k, j], (at.mirror(1), at.t)
+        )
+
+    def g_y2(k, j):
+        return remote(mx.at[k, j], yin2.at[k, j], sy2.at[k, j], ry2.at[k, j], at.y_dev(j))
+
+    cross = half // 2
+
+    def core_step(k, y_first):
         for j in range(ny):
             g_core(k, j).wait_recv()
             mine = gp[k, at.tp_of(at.y_peer(j), at.c)].astype(F32)
             gsum[k, j] = (mine + gin[k, j].astype(F32)).astype(BF)
-            if j:
-                g_y(k, j).start()
+            if y_first:
+                if j:
+                    g_y(k, j).start()
+            else:
+
+                @pl.when(lax.rem(k, 2) == 1)
+                def _():
+                    g_x2(lax.div(k, 2), j).start()
 
     def y_step(k):
         total = gsum[k, 0].astype(F32)
@@ -555,11 +579,34 @@
             total = total + yin[k, j].astype(F32)
         gy[k] = total.astype(BF)
 
-    def down(i):
-        return n - 1 - i
-
-    loop(0, n, lambda i: outer(down(i)))
-    loop(0, n, lambda i: core_step(down(i)))
+    def y_pair(k):
+        y_step(2 * k + 1)
+        g_x(2 * k + 1).start()
+        y_step(2 * k)
+
+    def x_step(k):
+        g_x(2 * k + 1).wait_recv()
+        gx[k] = (gy[2 * k].astype(F32) + xin[2 * k + 1].astype(F32)).astype(BF)
+        g_z(k).start()
+
+    def x2_step(k):
+        for j in range(ny):
+            g_x2(k, j).wait_recv()
+            both = gsum[2 * k, j].astype(F32) + xin2[k, j].astype(F32)
+            mx[k, j] = both.astype(BF)
+            if j:
+                g_y2(k, j).start()
+
+    def y2_step(k):
+        total = mx[k, 0].astype(F32)
+        for j in range(1, ny):
+            g_y2(k, j).wait_recv()
+            total = total + yin2[k, j].astype(F32)
+        return total
+
+    def y2_send(k):
+        gx[k] = y2_step(k).astype(BF)
+        g_z(k).start()
 
     def wide_tile(d):
         per = cols // min(256, cols)
@@ -570,15 +617,39 @@
         st_gate[out, :] = dot(tokens, dg[...], 0, 0).astype(BF)
         st_up[out, :] = dot(tokens, du[...], 0, 0).astype(BF)
 
-    loop(0, width // min(256, cols), wide_tile)
-    outs = [
-        pltpu.make_async_copy(st_gate, o_gate, o_sem.at[0]),
-        pltpu.make_async_copy(st_up, o_up, o_sem.at[1]),
-        pltpu.make_async_copy(st_down, o_down, o_sem.at[2]),
-    ]
-    outs[0].start()
-    outs[1].start()
-
+    def down_tile(f):
+        fs = part(f, ftile)
+        left = act[:, fs]
+        for b in range(nt):
+            bs = slice(b * cols, (b + 1) * cols)
+            st_down[fs, bs] = dot(left, inb[b, :, cols : 2 * cols], 0, 0).astype(BF)
+
+    outer(n - 1)
+    outer(n // 2 - 1)
+
+    def outer_high(i):
+        outer(n - 2 - i)
+        core_step(n - 1 - i, True)
+
+    def outer_low(i):
+        outer(half - 2 - i)
+        core_step(half - 1 - i, False)
+
+    def outer_both(i):
+        outer_high(i)
+        outer_low(i)
+
+    loop(0, half - 1, outer_both)
+    core_step(half, True)
+    core_step(0, False)
+
+    def tiles(lo, hi):
+        count = width // min(256, cols)
+        loop(lo * count // 8, hi * count // 8, wide_tile)
+
+    y_pair(half - 1)
+    x2_step(cross - 1)
+    tiles(0, 2)
     def ret_here(i):
         for j in range(ny):
             ret_copy(i, j).wait_recv()
@@ -603,20 +674,15 @@
         return remote(link, links.at[i], sk.at[i], rk.at[i], (at.mirror(i), at.t))
 
     loop(1, n, lambda i: link_copy(i).start())
-
-    loop(0, n, lambda i: y_step(down(i)))
-    loop(0, half, lambda k: g_x(2 * (half - 1 - k) + 1).start())
-
-    def down_tile(f):
-        fs = part(f, ftile)
-        left = act[:, fs]
-        for b in range(nt):
-            bs = slice(b * cols, (b + 1) * cols)
-            st_down[fs, bs] = dot(left, inb[b, :, cols : 2 * cols], 0, 0).astype(BF)
-
-    loop(0, hidden // ftile, down_tile)
-    outs[2].start()
-
+    x_step(half - 1)
+    for k in range(1, half - cross):
+        y_pair(half - 1 - k)
+        x2_step(cross - 1 - k)
+        y2_send(cross - k)
+        tiles(2, 5) if k == 1 else None
+        x_step(half - 1 - k)
+    tiles(5, 8)
+    o_proj[...] = y2_step(0)
     loop(1, n, lambda i: link_copy(i).wait_recv())
     links[0] = link[...]
 
@@ -631,17 +697,10 @@
     d_in = (adjoint * coef[3]).astype(BF)
     o_rec[...] = adjoint * coef[4] + dot(diagonal(rgate), d_rec) + dot(diagonal(igate), d_in)
 
-    def x_step(i):
+    loop(0, hidden // ftile, down_tile)
+
+    def z_step(i):
         k = half - 1 - i
-        g_x(2 * k + 1).wait_recv()
-        gx[k] = (gy[2 * k].astype(F32) + xin[2 * k + 1].astype(F32)).astype(BF)
-
-    loop(0, half, x_step)
-    loop(0, half - 1, lambda i: g_z(half - 1 - i).start())
-    o_proj[...] = gx[0].astype(F32)
-
-    def z_step(i):
-        k = i + 1
         g_z(k).wait_recv()
         o_proj[...] += zin[k].astype(F32)
 
@@ -650,8 +709,11 @@
     def drain(i):
         link_copy(i).wait_send()
         m_first(i).wait_send()
-        first(i, 0).wait_send()
         across(i, 0, True).wait_send()
+        @pl.when((i < far_1) | (i >= far_2))
+        def _():
+            first(i, 0).wait_send()
+
         for j in range(1, ny):
             across(i, j, True).wait_send()
 
@@ -681,25 +743,35 @@
     def drain_sums(k):
         for j in range(ny):
             g_core(k, j).wait_send()
+
+    loop(0, n, drain_sums)
+
+    def drain_high(k):
+        for j in range(1, ny):
+            g_y(2 * k, j).wait_send()
+            g_y(2 * k + 1, j).wait_send()
+        g_x(2 * k + 1).wait_send()
+
+    def drain_low(k):
+        for j in range(ny):
+            g_x2(k, j).wait_send()
             if j:
-                g_y(k, j).wait_send()
-
-    loop(0, n, drain_sums)
-    loop(0, half, lambda k: g_x(2 * k + 1).wait_send())
+                g_y2(k, j).wait_send()
+
+    loop(cross, half, drain_high)
+    loop(0, cross, drain_low)
     loop(1, half, lambda k: g_z(k).wait_send())
-    for copy in outs:
-        copy.wait()
 
 
 def fused(args, n, nt):
     (stream, cot, ids, rw, wg, wu, wd, op, mixed, rec_in, branch, before, rgate, igate, dparam, dshift) = args
     tok, width = cot.shape
-    top = ids.shape[1]
+    top = ids.shape[0]
     local_experts, _, hidden = wg.shape
     assert local_experts == 1
     rows = 2 * tok * top // n
     total, ny, cols, wl, blk, half = n * rows, nt // CORES, width // nt, op.shape[1], width // n, n // 2
-    head_dim = rgate.shape[1]
+    head_dim, cross = rgate.shape[1], half // 2
     channels = wl
     dma = pltpu.SemaphoreType.DMA
 
@@ -721,21 +793,30 @@
         buf(nt, hidden, wl), buf(nt, hidden, wl),
         buf(n, nt, blk, wl), buf(n, ny, blk, wl), buf(n, ny, blk, wl), buf(n, ny, blk, wl),
         buf(n, blk, wl), buf(n, blk, wl), buf(half, blk, wl), buf(half, blk, wl),
-        buf(width, hidden), buf(width, hidden), buf(hidden, width),
+        buf(cross, ny, blk, wl), buf(cross, ny, blk, wl), buf(cross, ny, blk, wl),
         buf(depth, wl, tok, dtype=F32), buf(7, wl, tok, dtype=F32),
         buf(8, wl, dtype=F32), buf(n, 8, wl, dtype=F32),
         buf(tok, wl), buf(tok, wl, dtype=F32), buf(wl, tok, dtype=F32), buf(width, wl, dtype=F32),
-        dma((4,)),
+        buf(tok, width), buf(tok, width), buf(top, tok, dtype=jnp.int32), buf(top, tok, dtype=F32),
+        buf(wl, tok), buf(wl, tok), buf(wl, tok), buf(wl, tok, dtype=F32),
+        buf(wl, head_dim), buf(wl, head_dim), buf(1, wl, dtype=F32), buf(wl, tok, dtype=F32),
+        dma((16,)),
         dma((n, ny)), dma((n, ny)), dma((n, ny)), dma((n, ny)), dma((n, ny)), dma((n, ny)),
         dma((n,)), dma((n,)), dma((ny,)), dma((ny,)), dma((ny,)), dma((ny,)),
         dma((ny,)), dma((ny,)), dma((ny,)), dma((ny,)),
         dma((3, ny)), dma((3, ny)), dma((n, ny)), dma((n, ny)), dma((n,)), dma((n,)),
         dma((n, ny)), dma((n, ny)), dma((n, ny)), dma((n, ny)),
-        dma((n,)), dma((n,)), dma((half,)), dma((half,)), dma((3,)),
+        dma((n,)), dma((n,)), dma((half,)), dma((half,)),
+        dma((cross, ny)), dma((cross, ny)), dma((cross, ny)), dma((cross, ny)),
     ]
+    operands = (
+        stream, cot, ids, rw, wg[0], wu[0], wd[0], op, mixed, rec_in, branch, before,
+        rgate.reshape(-1, head_dim), igate.reshape(-1, head_dim), dparam[None], dshift,
+    )
+    kept = 6 * width * hidden + 4 * blk * wl + 8 * wl * tok + MIB
     vm = pl.BlockSpec(memory_space=pltpu.VMEM)
-    hb = pl.BlockSpec(memory_space=pl.ANY)
-    shape = jax.ShapeDtypeStruct
+    hb = pl.BlockSpec(memory_space=pltpu.HBM)
+    shape = pltpu.VMEM
     return pl.pallas_call(
         functools.partial(fused_kernel, n, nt, head_dim),
         out_shape=(
@@ -746,21 +827,42 @@
             shape((channels, tok), F32),
             shape((channels, tok), F32),
         ),
-        in_specs=[vm] * 4 + [hb] * 4 + [vm] * 8,
-        out_specs=[hb] * 3 + [vm] * 3,
+        in_specs=[hb] * 16,
+        out_specs=[vm] * 6,
         scratch_shapes=scratch,
         compiler_params=pltpu.CompilerParams(
-            collective_id=0, has_side_effects=True, vmem_limit_bytes=VMEM_LIMIT
+            collective_id=0, has_side_effects=True, vmem_limit_bytes=62 * MIB - kept
         ),
-    )(
-        stream, cot, ids, rw, wg[0], wu[0], wd[0], op, mixed, rec_in, branch, before,
-        rgate.reshape(-1, head_dim), igate.reshape(-1, head_dim), dparam[None], dshift,
-    )
+    )(*[pltpu.with_memory_space_constraint(x, pltpu.HBM) for x in operands])
+
+
+def store_kernel(count, *refs):
+    sem = refs[-1]
+    copies = [
+        pltpu.make_async_copy(refs[i], refs[count + i], sem.at[i]) for i in range(count)
+    ]
+    for copy in copies:
+        copy.start()
+    for copy in copies:
+        copy.wait()
+
+
+def store(values):
+    count = len(values)
+    return pl.pallas_call(
+        functools.partial(store_kernel, count),
+        out_shape=[jax.ShapeDtypeStruct(v.shape, v.dtype) for v in values],
+        in_specs=[pl.BlockSpec(memory_space=pltpu.VMEM)] * count,
+        out_specs=[pl.BlockSpec(memory_space=pltpu.HBM)] * count,
+        scratch_shapes=[pltpu.SemaphoreType.DMA((count,))],
+        compiler_params=pltpu.CompilerParams(vmem_limit_bytes=16 * MIB),
+    )(*values)
 
 
 def local(*args):
     n, nt = lax.axis_size("sp"), lax.axis_size("tp")
-    gate, up, down, proj, rec, branch = fused(args, n, nt)
+    args = args[:2] + (args[2].T, args[3].T) + args[4:]
+    gate, up, down, proj, rec, branch = store(fused(args, n, nt))
     return gate[None], up[None], down[None], proj, rec, branch
 
 

time: 109 us -> 69.5 us (0.64)
  Pallas kernels: 96.3 us -> 68.7 us
  local copies, waits for them, and re-layouts: 11.6 us -> 0 us
    pallas_call x1, Pallas kernels: 96.3 us -> 66 us  [fused(): pl.pallas_call(functools.partial(fused_kernel, n, nt, head_dim), out_shap...]
    unnamed x18 -> x0, local copies, waits for them, and re-layouts: 11.6 us -> none
    pallas_call x0 -> x1, Pallas kernels: none -> 2.76 us  [store(): pl.pallas_call(functools.partial(store_kernel, count), out_shape=[jax.Sha...]
where the time goes in v2:
time: 69.5 us; the launch traced here: 69.4 us
  Pallas kernels  68.7 us (99%)
    pallas_call x1, Pallas kernels, fused(): pl.pallas_call(functools.partial(fused_kernel, n, nt, head_dim), out_shap...  66 us
    pallas_call x1, Pallas kernels, store(): pl.pallas_call(functools.partial(store_kernel, count), out_shape=[jax.Sha...  2.76 us

profile of v2, /device:TPU:0, one launch (start us, length us, event | category | flops | bytes accessed | tf_op | source)
XLA Modules:
  0.0 69.4 jit_solution(6783936182535639044)
XLA Ops:
  0.6 66.0 %shard_map.199 = (bf16[2048,512]{1,0:T(8,128)(2,1)S(1)}, bf16[2048,512]{1,0:T(8,128)(2,1)S(1)}, bf16[512,2048]{1,0:T(8,128)(2,1)S(1)}, f32[256,128]{1,0:T(8,128)...) custom-call(bf16[128,2048]{1,0:T(8,128)(2,1)} %refs_0_.1, bf16[128,2048]{1,0:T(8,128)(2,1)} %refs_1_.1, ...), custom_call_target="tpu_custom_call" | custom-call | tf_op jit(solution)/shard_map/pallas_call | solution.py:820
  66.6 2.8 %shard_map.200 = (bf16[2048,512]{1,0:T(8,128)(2,1)}, bf16[2048,512]{1,0:T(8,128)(2,1)}, bf16[512,2048]{1,0:T(8,128)(2,1)}, f32[256,128]{1,0:T(8,128)}, f32[128,128]{1,0:T(8,128)}, /*index=5*/f32[128,128]{1,0:T(8,128)}) custom-call(bf16[2048,512]{1,0:T(8,128)(2,1)S(1)} %get-tuple-element.18.refs_0_, bf16[2048,512]{1,0:T(8,128)(2,1)S(1)} %get-tuple-element.19.refs_1_, ...), custom_call_target="tpu_custom_call" | custom-call | tf_op jit(solution)/shard_map/pallas_call | solution.py:852

commit v3 on v2

--- a/solution.py
+++ b/solution.py
@@ -65,6 +65,7 @@
         self.partner = (self.s, self.y * CORES + 1 - self.c)
         quarter = n_sp // 4
         self.far = (2 * quarter, 3 * quarter)
+        self.inner = lax.rem(self.s // quarter + self.s // (2 * quarter), 2) == 1
 
     def mirror(self, i):
         found, bit = 0, 1
@@ -115,7 +116,10 @@
     half = n // 2
     quarter = n // 4
     groups = [list(range(nt))] if wl % 128 == 0 else [[b] for b in range(nt)]
-    ftile = min(256, hidden)
+    ftile, cross = min(256, hidden), half // 2
+    far_1, far_2 = at.far
+    near_rows, far_rows = half * rows, quarter * rows
+    far_a, far_b = far_1 * rows, far_2 * rows
 
     def cat(ref, sl, group):
         parts = [ref[b, sl, :] for b in group]
@@ -124,6 +128,9 @@
     def spread(value, group, put):
         for at_b, b in enumerate(group):
             put(b, value[:, at_b * wl : (at_b + 1) * wl])
+
+    def settle(ref, sem):
+        pltpu.make_async_copy(ref, ref, sem).wait()
 
     def loop(lo, hi, body):
         def step(i, carry):
@@ -212,22 +219,22 @@
     for j in range(ny):
         to_slots(1, half, at.q(j), put_src(j))
 
-    def first(i, j):
+    def first(i, j, phase=0):
         return remote(
             src.at[j, part(i, rows), :],
             inb.at[at.q(j), part(i, rows), :],
-            s1.at[i, j],
-            r1.at[i, j],
+            s1.at[phase],
+            r1.at[i],
             (at.mirror(i), at.t),
         )
 
     def along_y(i, j, outgoing):
         spot = inb.at[at.t if outgoing else at.q(j), part(i, rows), :]
-        return remote(spot, spot, sy.at[i, j], ry.at[i, j], at.y_dev(j))
-
-    def across(i, j, outgoing):
-        spot = inb.at[at.q(j, outgoing), part(i, rows), :]
-        return remote(spot, spot, sx.at[i, j], rx.at[i, j], at.partner)
+        return remote(spot, spot, sy.at[0], ry.at[i - half, j], at.y_dev(j))
+
+    def across(i, j, group):
+        spot = inb.at[at.q(j), part(i, rows), :]
+        return remote(spot, spot, sx.at[0], rx.at[group], at.partner)
 
     def op_y(j, outgoing):
         spot = opf.at[at.t if outgoing else at.q(j)]
@@ -241,8 +248,8 @@
         return remote(
             msrc.at[part(i, rows), :],
             mb.at[at.t, part(i, rows), :],
-            sm.at[i],
-            rm.at[i],
+            sm.at[0],
+            rm.at[0],
             (at.mirror(i), at.t),
         )
 
@@ -277,9 +284,11 @@
         to_slots(0, 1, tp, put)
 
     loop(0, nt, own_slots)
-    far_1, far_2 = at.far
-    loop(far_1, far_2, lambda i: first(i, 0).start())
+    loop(far_1, far_2, lambda i: first(i, 0, 1).start())
     mb[at.t, 0:rows, :] = msrc[0:rows, :]
+    loop(split, half, send_near)
+    loop(far_2, n, lambda i: first(i, 0, 2).start())
+    loop(1, n, lambda i: m_first(i).start())
 
     lane_w = lax.broadcasted_iota(jnp.int32, (wl, wl), 1)
     sub_w = lax.broadcasted_iota(jnp.int32, (wl, wl), 0)
@@ -351,26 +360,31 @@
         copy.wait()
 
     def near_in(i):
+        settle(src.at[:, 0:rows, :], r1.at[i])
         for j in range(ny):
-            first(i, j).wait_recv()
-            across(i, j, True).start()
-
-    def far_in(i):
-        first(i, 0).wait_recv()
-        for j in range(1, ny):
-            along_y(i, j, True).start()
-        across(i, 0, True).start()
-
-    def far_pass(i):
-        for j in range(1, ny):
-            along_y(i, j, False).wait_recv()
-            across(i, j, True).start()
-
-    def all_here(i):
-        for j in range(ny):
-            across(i, j, False).wait_recv()
-
-    def forward(r0, size):
+            across(i, j, 0).start()
+
+    def far_in(group):
+        def one(i):
+            first(i, 0).wait_recv()
+            for j in range(1, ny):
+                along_y(i, j, True).start()
+            across(i, 0, group).start()
+
+        return one
+
+    def far_pass(group):
+        def one(i):
+            for j in range(1, ny):
+                along_y(i, j, False).wait_recv()
+                across(i, j, group).start()
+
+        return one
+
+    def all_here(group, lo, hi):
+        settle(inb.at[0:ny, lo * rows : hi * rows, :], rx.at[group])
+
+    def forward(r0, size, lo=0, hi=hidden // ftile):
         rs = pl.ds(r0, size)
 
         def tile(f):
@@ -391,7 +405,7 @@
             dg[rs, fs] = jnp.where(gate > CLAMP_LIMIT, 0.0, d_act * curve).astype(BF)
             du[rs, fs] = jnp.where(jnp.abs(up) > CLAMP_LIMIT, 0.0, d_act * gs).astype(BF)
 
-        loop(0, hidden // ftile, tile)
+        loop(lo, hi, tile)
 
     def project(r0, size):
         rs = pl.ds(r0, size)
@@ -409,17 +423,17 @@
         return remote(
             q.at[at.tp_of(yj, 1 - at.c), pl.ds(r0, size), :],
             qin.at[j, pl.ds(r0, size), :],
-            sq.at[g, j],
+            sq.at[0],
             rq.at[g, j],
             at.partner,
         )
 
-    def ret_copy(i, j):
+    def ret_copy(i, j, own=0):
         return remote(
             qsum.at[j, part(i, rows), :],
             ret.at[j, part(i, rows), :],
-            sr.at[i, j],
-            rr.at[i, j],
+            sr.at[own],
+            rr.at[own],
             at.dev(i, j),
         )
 
@@ -452,53 +466,53 @@
 
                 spread(value, group, put)
 
-    near_rows = half * rows
-    far_rows = quarter * rows
-    far_a, far_b = far_1 * rows, far_2 * rows
     near_in(1)
-    loop(far_1, far_2, lambda i: first(i, 0).wait_send())
-    loop(split, half, send_near)
-    loop(far_2, n, lambda i: first(i, 0).start())
-    loop(1, n, lambda i: m_first(i).start())
     loop(2, split, near_in)
     for j in range(1, ny):
         op_y(j, False).wait_recv()
         op_x(j, True).start()
-    loop(far_1, far_2, far_in)
+    loop(far_1, far_2, far_in(1))
     for j in range(ny):
         op_x(j, False).wait_recv()
     loop(0, hidden // ftile, weight_maps)
-    loop(far_1, far_2, far_pass)
+    loop(far_1, far_2, far_pass(1))
     loop(split, half, near_in)
-    loop(far_2, n, far_in)
-    loop(1, half, all_here)
+
+    @pl.when(at.inner)
+    def _():
+        loop(far_2, n, far_in(2))
+
+    all_here(0, 1, half)
     forward(0, near_rows)
     project(0, near_rows)
     q_send(0, 0, near_rows)
-    loop(1, n, lambda i: m_first(i).wait_recv())
+
+    @pl.when(jnp.logical_not(at.inner))
+    def _():
+        loop(far_2, n, far_in(2))
+
+    all_here(1, far_1, far_2)
+    settle(msrc.at[rows:, :], rm.at[0])
     for j in range(1, ny):
         m_y(j, True).start()
     m_x(0, True).start()
-    loop(far_1, far_2, all_here)
     forward(far_a, far_rows)
     project(far_a, far_rows)
     q_send(1, far_a, far_rows)
-    loop(far_2, n, far_pass)
+    loop(far_2, n, far_pass(2))
     q_reduce(0, 0, near_rows)
     q_reduce(1, far_a, far_rows)
     ret[0, 0:rows, :] = qsum[0, 0:rows, :]
     for j in range(1, ny):
-        ret_copy(0, j).start()
+        ret_copy(0, j, 1).start()
     loop(1, far_2, ret_send)
-    loop(far_2, n, all_here)
+    all_here(2, far_2, n)
     forward(far_b, far_rows)
-    project(far_b, far_rows)
-    q_send(2, far_b, far_rows)
     for j in range(1, ny):
         m_y(j, False).wait_recv()
         m_x(j, True).start()
-    q_reduce(2, far_b, far_rows)
-    loop(far_2, n, ret_send)
+    project(far_b, far_rows)
+    q_send(2, far_b, far_rows)
     for j in range(ny):
         m_x(j, False).wait_recv()
 
@@ -515,13 +529,15 @@
                 spread(value, group, put)
 
     loop(0, hidden // ftile, inner)
+    q_reduce(2, far_b, far_rows)
+    loop(far_2, n, ret_send)
 
     def g_core(k, j):
         return remote(
             gp.at[k, at.tp_of(at.y_peer(j), 1 - at.c)],
             gin.at[k, j],
-            sg.at[k, j],
-            rg.at[k, j],
+            sg.at[0],
+            rg.at[k],
             at.partner,
         )
 
@@ -540,27 +556,26 @@
             g_core(k, j).start()
 
     def g_y(k, j):
-        return remote(gsum.at[k, j], yin.at[k, j], sgy.at[k, j], rgy.at[k, j], at.y_dev(j))
+        return remote(gsum.at[k, j], yin.at[k, j], sgy.at[0], rgy.at[k - half, j], at.y_dev(j))
 
     def g_x(k):
-        return remote(gy.at[k], xin.at[k], sgx.at[k], rgx.at[k], (at.mirror(1), at.t))
+        h = lax.div(k, 2)
+        return remote(gy.at[k], xin.at[h], sgx.at[0], rgx.at[h - cross], (at.mirror(1), at.t))
 
     def g_z(k):
-        return remote(gx.at[k], zin.at[k], sgz.at[k], rgz.at[k], (at.mirror(2 * k), at.t))
+        return remote(gx.at[k], zin.at[k], sgz.at[0], rgz.at[k], (at.mirror(2 * k), at.t))
 
     def g_x2(k, j):
         return remote(
-            gsum.at[2 * k + 1, j], xin2.at[k, j], sx2.at[k, j], rx2.at[k, j], (at.mirror(1), at.t)
+            gsum.at[2 * k + 1, j], xin2.at[k, j], sx2.at[0], rx2.at[k], (at.mirror(1), at.t)
         )
 
     def g_y2(k, j):
-        return remote(mx.at[k, j], yin2.at[k, j], sy2.at[k, j], ry2.at[k, j], at.y_dev(j))
-
-    cross = half // 2
+        return remote(mx.at[k, j], yin2.at[k, j], sy2.at[0], ry2.at[k, j], at.y_dev(j))
 
     def core_step(k, y_first):
+        settle(gin.at[k], rg.at[k])
         for j in range(ny):
-            g_core(k, j).wait_recv()
             mine = gp[k, at.tp_of(at.y_peer(j), at.c)].astype(F32)
             gsum[k, j] = (mine + gin[k, j].astype(F32)).astype(BF)
             if y_first:
@@ -586,12 +601,12 @@
 
     def x_step(k):
         g_x(2 * k + 1).wait_recv()
-        gx[k] = (gy[2 * k].astype(F32) + xin[2 * k + 1].astype(F32)).astype(BF)
+        gx[k] = (gy[2 * k].astype(F32) + xin[k].astype(F32)).astype(BF)
         g_z(k).start()
 
     def x2_step(k):
+        settle(xin2.at[k], rx2.at[k])
         for j in range(ny):
-            g_x2(k, j).wait_recv()
             both = gsum[2 * k, j].astype(F32) + xin2[k, j].astype(F32)
             mx[k, j] = both.astype(BF)
             if j:
@@ -647,16 +662,13 @@
         count = width // min(256, cols)
         loop(lo * count // 8, hi * count // 8, wide_tile)
 
+    tiles(0, 2)
     y_pair(half - 1)
     x2_step(cross - 1)
-    tiles(0, 2)
-    def ret_here(i):
-        for j in range(ny):
-            ret_copy(i, j).wait_recv()
-
-    for j in range(1, ny):
-        ret_copy(0, j).wait_recv()
-    loop(1, n, ret_here)
+    loop(1, half - cross, lambda i: y_pair(half - 1 - i))
+    settle(ret.at[:, rows:, :], rr.at[0])
+    if ny > 1:
+        settle(ret.at[1:, 0:rows, :], rr.at[1])
     total = dm0[...]
     for j in range(ny):
         total = total + dot(land_t[...], ret[j])
@@ -671,19 +683,19 @@
     link[1:2, :] = to_row(coef[6][:, 0:1] * run[:, 0:1])
 
     def link_copy(i):
-        return remote(link, links.at[i], sk.at[i], rk.at[i], (at.mirror(i), at.t))
+        return remote(link, links.at[i], sk.at[0], rk.at[0], (at.mirror(i), at.t))
 
     loop(1, n, lambda i: link_copy(i).start())
+    tiles(2, 4)
+    loop(1, cross, lambda i: x2_step(cross - 1 - i))
     x_step(half - 1)
-    for k in range(1, half - cross):
-        y_pair(half - 1 - k)
-        x2_step(cross - 1 - k)
-        y2_send(cross - k)
-        tiles(2, 5) if k == 1 else None
-        x_step(half - 1 - k)
+    loop(0, cross - 1, lambda i: y2_send(cross - 1 - i))
+    tiles(4, 5)
+    loop(1, half - cross, lambda i: x_step(half - 1 - i))
     tiles(5, 8)
     o_proj[...] = y2_step(0)
-    loop(1, n, lambda i: link_copy(i).wait_recv())
+    loop(0, hidden // ftile, down_tile)
+    settle(links.at[1:], rk.at[0])
     links[0] = link[...]
 
     def compose(k, carry):
@@ -697,8 +709,6 @@
     d_in = (adjoint * coef[3]).astype(BF)
     o_rec[...] = adjoint * coef[4] + dot(diagonal(rgate), d_rec) + dot(diagonal(igate), d_in)
 
-    loop(0, hidden // ftile, down_tile)
-
     def z_step(i):
         k = half - 1 - i
         g_z(k).wait_recv()
@@ -706,61 +716,29 @@
 
     loop(0, half - 1, z_step)
 
-    def drain(i):
-        link_copy(i).wait_send()
-        m_first(i).wait_send()
-        across(i, 0, True).wait_send()
-        @pl.when((i < far_1) | (i >= far_2))
-        def _():
-            first(i, 0).wait_send()
-
-        for j in range(1, ny):
-            across(i, j, True).wait_send()
-
-            @pl.when(i < half)
-            def _():
-                first(i, j).wait_send()
-
-            @pl.when(i >= half)
-            def _():
-                along_y(i, j, True).wait_send()
-
-        for j in range(ny):
-            ret_copy(i, j).wait_send()
-
-    loop(1, n, drain)
+    settle(src.at[:, rows:near_rows, :], s1.at[0])
+    settle(src.at[0, far_b:, :], s1.at[2])
+    settle(src.at[0, far_a : far_a + far_rows, :], s1.at[1])
+    settle(inb.at[0:ny, rows:, :], sx.at[0])
+    settle(msrc.at[rows:, :], sm.at[0])
+    settle(qin, sq.at[0])
+    settle(qsum.at[:, rows:, :], sr.at[0])
+    settle(links.at[1:], sk.at[0])
+    settle(gin, sg.at[0])
+    settle(gx.at[cross:], sgx.at[0])
+    settle(zin.at[1:], sgz.at[0])
+    settle(xin2, sx2.at[0])
+    if ny > 1:
+        settle(inb.at[0 : ny - 1, near_rows:, :], sy.at[0])
+        settle(qsum.at[1:, 0:rows, :], sr.at[1])
+        settle(yin.at[half:, 1:], sgy.at[0])
+        settle(yin2.at[:, 1:], sy2.at[0])
     for j in range(1, ny):
-        ret_copy(0, j).wait_send()
         op_y(j, True).wait_send()
         m_y(j, True).wait_send()
     for j in range(ny):
         op_x(j, True).wait_send()
         m_x(j, True).wait_send()
-        q_core(0, 0, near_rows, j, True).wait_send()
-        q_core(1, far_a, far_rows, j, True).wait_send()
-        q_core(2, far_b, far_rows, j, True).wait_send()
-
-    def drain_sums(k):
-        for j in range(ny):
-            g_core(k, j).wait_send()
-
-    loop(0, n, drain_sums)
-
-    def drain_high(k):
-        for j in range(1, ny):
-            g_y(2 * k, j).wait_send()
-            g_y(2 * k + 1, j).wait_send()
-        g_x(2 * k + 1).wait_send()
-
-    def drain_low(k):
-        for j in range(ny):
-            g_x2(k, j).wait_send()
-            if j:
-                g_y2(k, j).wait_send()
-
-    loop(cross, half, drain_high)
-    loop(0, cross, drain_low)
-    loop(1, half, lambda k: g_z(k).wait_send())
 
 
 def fused(args, n, nt):
@@ -792,7 +770,7 @@
         buf(nt, total, wl), buf(ny, total, wl), buf(ny, total, wl), buf(ny, total, wl),
         buf(nt, hidden, wl), buf(nt, hidden, wl),
         buf(n, nt, blk, wl), buf(n, ny, blk, wl), buf(n, ny, blk, wl), buf(n, ny, blk, wl),
-        buf(n, blk, wl), buf(n, blk, wl), buf(half, blk, wl), buf(half, blk, wl),
+        buf(n, blk, wl), buf(half, blk, wl), buf(half, blk, wl), buf(half, blk, wl),
         buf(cross, ny, blk, wl), buf(cross, ny, blk, wl), buf(cross, ny, blk, wl),
         buf(depth, wl, tok, dtype=F32), buf(7, wl, tok, dtype=F32),
         buf(8, wl, dtype=F32), buf(n, 8, wl, dtype=F32),
@@ -801,13 +779,13 @@
         buf(wl, tok), buf(wl, tok), buf(wl, tok), buf(wl, tok, dtype=F32),
         buf(wl, head_dim), buf(wl, head_dim), buf(1, wl, dtype=F32), buf(wl, tok, dtype=F32),
         dma((16,)),
-        dma((n, ny)), dma((n, ny)), dma((n, ny)), dma((n, ny)), dma((n, ny)), dma((n, ny)),
-        dma((n,)), dma((n,)), dma((ny,)), dma((ny,)), dma((ny,)), dma((ny,)),
+        dma((3,)), dma((n,)), dma((1,)), dma((half, ny)), dma((1,)), dma((3,)),
+        dma((1,)), dma((1,)), dma((ny,)), dma((ny,)), dma((ny,)), dma((ny,)),
         dma((ny,)), dma((ny,)), dma((ny,)), dma((ny,)),
-        dma((3, ny)), dma((3, ny)), dma((n, ny)), dma((n, ny)), dma((n,)), dma((n,)),
-        dma((n, ny)), dma((n, ny)), dma((n, ny)), dma((n, ny)),
-        dma((n,)), dma((n,)), dma((half,)), dma((half,)),
-        dma((cross, ny)), dma((cross, ny)), dma((cross, ny)), dma((cross, ny)),
+        dma((1,)), dma((3, ny)), dma((2,)), dma((2,)), dma((1,)), dma((1,)),
+        dma((1,)), dma((n,)), dma((1,)), dma((n - half, ny)),
+        dma((1,)), dma((half - cross,)), dma((1,)), dma((half,)),
+        dma((1,)), dma((cross,)), dma((1,)), dma((cross, ny)),
     ]
     operands = (
         stream, cot, ids, rw, wg[0], wu[0], wd[0], op, mixed, rec_in, branch, before,

time: 69.5 us -> 65.9 us (0.948)
  Pallas kernels: 68.7 us -> 65.1 us
    pallas_call x1, Pallas kernels: 66 us -> 62.3 us  [fused(): pl.pallas_call(functools.partial(fused_kernel, n, nt, head_dim), out_shap...]
where the time goes in v3:
time: 65.9 us; the launch traced here: 65.7 us
  Pallas kernels  65.1 us (99%)
    pallas_call x1, Pallas kernels, fused(): pl.pallas_call(functools.partial(fused_kernel, n, nt, head_dim), out_shap...  62.3 us
    pallas_call x1, Pallas kernels, store(): pl.pallas_call(functools.partial(store_kernel, count), out_shape=[jax.Sha...  2.76 us

profile of v3, /device:TPU:0, one launch (start us, length us, event | category | flops | bytes accessed | tf_op | source)
XLA Modules:
  0.0 65.7 jit_solution(10175843126447373464)
XLA Ops:
  0.6 62.3 %shard_map.199 = (bf16[2048,512]{1,0:T(8,128)(2,1)S(1)}, bf16[2048,512]{1,0:T(8,128)(2,1)S(1)}, bf16[512,2048]{1,0:T(8,128)(2,1)S(1)}, f32[256,128]{1,0:T(8,128)...) custom-call(bf16[128,2048]{1,0:T(8,128)(2,1)} %refs_0_.1, bf16[128,2048]{1,0:T(8,128)(2,1)} %refs_1_.1, ...), custom_call_target="tpu_custom_call" | custom-call | tf_op jit(solution)/shard_map/pallas_call | solution.py:798
  63.0 2.8 %shard_map.200 = (bf16[2048,512]{1,0:T(8,128)(2,1)}, bf16[2048,512]{1,0:T(8,128)(2,1)}, bf16[512,2048]{1,0:T(8,128)(2,1)}, f32[256,128]{1,0:T(8,128)}, f32[128,128]{1,0:T(8,128)}, /*index=5*/f32[128,128]{1,0:T(8,128)}) custom-call(bf16[2048,512]{1,0:T(8,128)(2,1)S(1)} %get-tuple-element.18.refs_0_, bf16[2048,512]{1,0:T(8,128)(2,1)S(1)} %get-tuple-element.19.refs_1_, ...), custom_call_target="tpu_custom_call" | custom-call | tf_op jit(solution)/shard_map/pallas_call | solution.py:830

commit v4 on v3

--- a/solution.py
+++ b/solution.py
@@ -116,7 +116,7 @@
     half = n // 2
     quarter = n // 4
     groups = [list(range(nt))] if wl % 128 == 0 else [[b] for b in range(nt)]
-    ftile, cross = min(256, hidden), half // 2
+    ftile, cross = min(512, hidden), half // 2
     far_1, far_2 = at.far
     near_rows, far_rows = half * rows, quarter * rows
     far_a, far_b = far_1 * rows, far_2 * rows

time: 65.9 us -> 65.8 us (level)
  no operation moved by 1% of the time
where the time goes in v4:
time: 65.8 us; the launch traced here: 65.7 us
  Pallas kernels  64.9 us (99%)
  between operations  0.81 us (1%)
    pallas_call x1, Pallas kernels, fused(): pl.pallas_call(functools.partial(fused_kernel, n, nt, head_dim), out_shap...  62.1 us
    pallas_call x1, Pallas kernels, store(): pl.pallas_call(functools.partial(store_kernel, count), out_shape=[jax.Sha...  2.76 us

profile of v4, /device:TPU:0, one launch (start us, length us, event | category | flops | bytes accessed | tf_op | source)
XLA Modules:
  0.0 65.7 jit_solution(12216611690568958404)
XLA Ops:
  0.6 62.1 %shard_map.199 = (bf16[2048,512]{1,0:T(8,128)(2,1)S(1)}, bf16[2048,512]{1,0:T(8,128)(2,1)S(1)}, bf16[512,2048]{1,0:T(8,128)(2,1)S(1)}, f32[256,128]{1,0:T(8,128)...) custom-call(bf16[128,2048]{1,0:T(8,128)(2,1)} %refs_0_.1, bf16[128,2048]{1,0:T(8,128)(2,1)} %refs_1_.1, ...), custom_call_target="tpu_custom_call" | custom-call | tf_op jit(solution)/shard_map/pallas_call | solution.py:798
  62.7 2.8 %shard_map.200 = (bf16[2048,512]{1,0:T(8,128)(2,1)}, bf16[2048,512]{1,0:T(8,128)(2,1)}, bf16[512,2048]{1,0:T(8,128)(2,1)}, f32[256,128]{1,0:T(8,128)}, f32[128,128]{1,0:T(8,128)}, /*index=5*/f32[128,128]{1,0:T(8,128)}) custom-call(bf16[2048,512]{1,0:T(8,128)(2,1)S(1)} %get-tuple-element.18.refs_0_, bf16[2048,512]{1,0:T(8,128)(2,1)S(1)} %get-tuple-element.19.refs_1_, ...), custom_call_target="tpu_custom_call" | custom-call | tf_op jit(solution)/shard_map/pallas_call | solution.py:830
